TPU v7x, 32 devices: a whole 2x2x4 slice. The times are simulated.
32 devices in a mesh: sp: 4 (over z), tp: 4 (over y, x), dp: 2 (over core).
Axes of the slice: x: 2, y: 2, z: 4, core: 2. Of those that a mesh axis runs over, the one named last changes fastest.
Arguments:
- latent_tokens: bfloat16 [4096, 2048], P(('dp', 'sp', 'tp')), parts along dimension 0, may hold values from -6 to 6
- condition: bfloat16 [4096], P(('dp', 'sp')), parts along dimension 0, may hold values from -6 to 6
- shift_weight: bfloat16 [2048, 2048], P('sp', 'tp'), may hold values from -0.125 to 0.125
- scale_weight: bfloat16 [2048, 2048], P('sp', 'tp'), may hold values from -0.125 to 0.125
- gate_weight: bfloat16 [2048, 2048], P('sp', 'tp'), may hold values from -0.125 to 0.125
- norm_gain: float32 [2048], replicated, may hold values from 0.1 to 1.9
- query_down: bfloat16 [2048, 512], replicated, may hold values from -0.125 to 0.125
- query_gain: float32 [512], replicated, may hold values from 0.1 to 1.9
- kv_down: bfloat16 [2048, 256], replicated, may hold values from -0.125 to 0.125
- kv_gain: float32 [256], replicated, may hold values from 0.1 to 1.9
- rope_down: bfloat16 [2048, 32], replicated, may hold values from -0.125 to 0.125
- query_up: bfloat16 [512, 1536], P(None, 'tp'), may hold values from -0.25 to 0.25
- key_up: bfloat16 [256, 1024], P(None, 'tp'), may hold values from -0.375 to 0.375
- value_up: bfloat16 [256, 1024], P(None, 'tp'), may hold values from -0.375 to 0.375
- query_norm_gain: float32 [96], replicated, may hold values from 0.47 to 16
- key_norm_gain: float32 [96], replicated, may hold values from 0.47 to 16
- out_weight: bfloat16 [1024, 2048], P('tp'), may hold values from -0.1875 to 0.1875
- context_latent: bfloat16 [2048, 256], P(('dp', 'sp')), parts along dimension 0, may hold values from -6 to 6
- context_rope: bfloat16 [2048, 32], P(('dp', 'sp')), parts along dimension 0, may hold values from -6 to 6
- context_lift: float32 [16], P('tp'), may hold values from 0 to 2
Outputs:
- output: bfloat16 [4096, 2048], P(('dp', 'sp', 'tp')), parts along dimension 0
There are 2 independent parts, one for each index of `dp`. A program takes and returns all parts, laid end to end along the dimension named above; an argument that names none is the same for every part. Nothing has to cross between parts.
All inputs are finite; a program needn't handle non-finite values.
Results may differ from a plain program's by a relative error of at most 0.015.
The roundings to bfloat16 on the way count: a program that leaves them out, or rounds other values in their place, can miss the bound.
Values may be sent and summed in bfloat16 or wider, within the bound.
A program may use at most 128 MiB of HBM per device.

v0:
```python
import functools

import jax
import jax.numpy as jnp
import numpy as np
from jax import lax
from jax.experimental import pallas as pl
from jax.experimental.pallas import tpu as pltpu
from jax.sharding import PartitionSpec as P

NOPE_DIM = 64
ROPE_DIM = 32
VALUE_DIM = 64
QK_DIM = 96
GRID_W = 64
LANES = 128

EPS = 1e-06
THETA = 10000.0
LOG2E = 1.4426950408889634
MESH = pl.DeviceIdType.MESH
VMEM_SPEC = pl.BlockSpec(memory_space=pltpu.VMEM)
ANY_SPEC = pl.BlockSpec(memory_space=pl.ANY)
BF16 = jnp.bfloat16
F32 = jnp.float32


def partner_order():
    return np.arange(ROPE_DIM) ^ (ROPE_DIM // 4)


def rope_spread():
    spread = np.zeros((ROPE_DIM, LANES), np.float32)
    order = partner_order()
    for j in range(ROPE_DIM):
        spread[j, NOPE_DIM + j] = 1.0
        spread[order[j], QK_DIM + j] = 1.0
    return spread


def query_spread(heads):
    spread = np.zeros((heads * QK_DIM, heads * LANES), np.float32)
    order = partner_order()
    for h in range(heads):
        for j in range(QK_DIM):
            spread[h * QK_DIM + j, h * LANES + j] = 1.0
        for j in range(ROPE_DIM):
            spread[h * QK_DIM + NOPE_DIM + order[j], h * LANES + QK_DIM + j] = 1.0
    return spread


def head_spread(heads, width):
    spread = np.zeros((heads * width, heads * LANES), np.float32)
    for h in range(heads):
        for j in range(width):
            spread[h * width + j, h * LANES + j] = 1.0
    return spread


def turn_tables(count, axis):
    freq_count = ROPE_DIM // 4
    inverse = np.float32(THETA) ** (-np.float32(4.0) * np.arange(freq_count, dtype=np.float32) / np.float32(ROPE_DIM))
    angles = np.arange(count, dtype=np.float32)[:, None] * inverse.astype(np.float32)
    cosine = np.zeros((count, LANES), np.float32)
    sine = np.zeros((count, LANES), np.float32)
    start = NOPE_DIM + axis * 2 * freq_count
    mid = start + freq_count
    cosine[:, start:mid] = np.cos(angles.astype(np.float64))
    cosine[:, mid : mid + freq_count] = np.cos(angles.astype(np.float64))
    sine[:, start:mid] = -np.sin(angles.astype(np.float64))
    sine[:, mid : mid + freq_count] = np.sin(angles.astype(np.float64))
    if axis == 0:
        cosine[:, :NOPE_DIM] = 1.0
    return cosine, sine


def norm_factor(values):
    return lax.rsqrt(jnp.mean(values * values, axis=-1, keepdims=True) + EPS)


def front_kernel(
    sp, tp,
    cond_ref, shift_hbm, scale_hbm, gate_hbm, tokens_hbm, gain_ref, qd_hbm, qg_ref, kd_hbm, kg_ref, rd_ref,
    cl_ref, cr_ref, spread_ref,
    q_out, kv_out, ctx_out, gate_out,
    mods, q_own, kv_own, ctx_own,
    mod_send, mod_recv, q_send, q_recv, kv_send, kv_recv, c_send, c_recv, local_sem,
    shift_w, scale_w, gate_w, tokens_ref, qd_ref, kd_ref, load_sem,
):
    loads = []
    for i, (src, dst) in enumerate((
        (shift_hbm, shift_w), (scale_hbm, scale_w), (gate_hbm, gate_w),
        (tokens_hbm, tokens_ref), (qd_hbm, qd_ref), (kd_hbm, kd_ref),
    )):
        loads.append(pltpu.make_async_copy(src, dst, load_sem.at[i]))
        loads[-1].start()
    s_me = lax.axis_index("sp")
    t_me = lax.axis_index("tp")
    me = s_me * tp + t_me
    half = mods.shape[2]
    rank = cl_ref.shape[1]

    def peer(ds, dt):
        return lax.rem(s_me + ds, sp), lax.rem(t_me + dt, tp)

    others = [(ds, dt) for ds in range(sp) for dt in range(tp) if ds or dt]
    barrier = pltpu.get_barrier_semaphore()
    for ds, dt in others:
        ps, pt = peer(ds, dt)
        pl.semaphore_signal(barrier, inc=1, device_id={"sp": ps, "tp": pt}, device_id_type=MESH)

    c = cond_ref[...].astype(F32)
    act = (c / (1.0 + jnp.exp(-c))).astype(BF16)
    act = jnp.broadcast_to(act, (16, act.shape[1]))
    rows = []
    for i, w in enumerate((shift_w, scale_w, gate_w)):
        loads[i].wait()
        term = jnp.dot(act, w[...], preferred_element_type=F32)[0:1]
        rows += [term[:, :half], term[:, half:]]
    mods[me] = jnp.concatenate(rows + [rows[0], rows[0]], axis=0)

    spread = spread_ref[...]
    ctx_own[:, :rank] = cl_ref[...]
    ctx_own[:, rank:] = lax.dot_general(
        cr_ref[...], spread, (((0,), (0,)), ((), ())), preferred_element_type=F32
    ).astype(BF16)

    pl.semaphore_wait(barrier, len(others))
    copies = []
    mod_copies = []
    for i, (ds, dt) in enumerate(others):
        ps, pt = peer(ds, dt)
        cp = pltpu.make_async_remote_copy(
            src_ref=mods.at[me], dst_ref=mods.at[me], send_sem=mod_send.at[i], recv_sem=mod_recv.at[i],
            device_id={"sp": ps, "tp": pt}, device_id_type=MESH,
        )
        cp.start()
        mod_copies.append(cp)
    for ds in range(1, sp):
        ps, pt = peer(ds, 0)
        cp = pltpu.make_async_remote_copy(
            src_ref=ctx_own, dst_ref=ctx_out.at[s_me], send_sem=c_send.at[ds - 1], recv_sem=c_recv.at[ds - 1],
            device_id={"sp": ps, "tp": pt}, device_id_type=MESH,
        )
        cp.start()
        copies.append(cp)
    own = [pltpu.make_async_copy(ctx_own, ctx_out.at[s_me], local_sem.at[0])]
    own[0].start()

    for load in loads[3:]:
        load.wait()
    x = tokens_ref[...].astype(F32)
    xn = x * norm_factor(x) * gain_ref[...]

    for cp in mod_copies:
        cp.wait_recv()
    pieces = [[], [], []]
    for t in range(tp):
        total = mods[t]
        for s in range(1, sp):
            total = total + mods[s * tp + t]
        for k in range(3):
            pieces[k] += [total[2 * k : 2 * k + 1], total[2 * k + 1 : 2 * k + 2]]
    shift, scale, gate = [jnp.concatenate(p, axis=1) for p in pieces]
    gate_out[...] = gate
    normed = (xn * (1.0 + scale) + shift).astype(BF16)

    q = jnp.dot(normed, qd_ref[...], preferred_element_type=F32)
    q_own[...] = (q * norm_factor(q) * qg_ref[...]).astype(BF16)
    kv = jnp.dot(normed, kd_ref[...], preferred_element_type=F32)
    kv_own[:, :rank] = (kv * norm_factor(kv) * kg_ref[...]).astype(BF16)
    rope = lax.dot_general(
        normed, rd_ref[...], (((1,), (1,)), ((), ())), preferred_element_type=F32
    ).astype(BF16)
    kv_own[:, rank:] = jnp.dot(rope, spread, preferred_element_type=F32).astype(BF16)

    for dt in range(1, tp):
        ps, pt = peer(0, dt)
        cp = pltpu.make_async_remote_copy(
            src_ref=q_own, dst_ref=q_out.at[t_me], send_sem=q_send.at[dt - 1], recv_sem=q_recv.at[dt - 1],
            device_id={"sp": ps, "tp": pt}, device_id_type=MESH,
        )
        cp.start()
        copies.append(cp)
    for i, (ds, dt) in enumerate(others):
        ps, pt = peer(ds, dt)
        cp = pltpu.make_async_remote_copy(
            src_ref=kv_own, dst_ref=kv_out.at[me], send_sem=kv_send.at[i], recv_sem=kv_recv.at[i],
            device_id={"sp": ps, "tp": pt}, device_id_type=MESH,
        )
        cp.start()
        copies.append(cp)
    own.append(pltpu.make_async_copy(q_own, q_out.at[t_me], local_sem.at[1]))
    own.append(pltpu.make_async_copy(kv_own, kv_out.at[me], local_sem.at[2]))
    own[1].start()
    own[2].start()
    for cp in mod_copies:
        cp.wait_send()
    for cp in copies:
        cp.wait()
    for cp in own:
        cp.wait()


def attend_kernel(
    heads, s_ref, q_ref, kv_ref, ctx_ref, qu_ref, ku_ref, vu_ref, qe_ref, ke_ref, ve_ref,
    qgain_ref, kgain_ref, lift_ref, row_a, row_b, col_a, col_b, out_ref,
    k_lat, v_lat, k_ctx, v_ctx, q_all,
):
    rank = ku_ref.shape[0]
    tokens = kv_ref.shape[0]
    group = q_ref.shape[0]
    context = ctx_ref.shape[0]
    lane = lax.broadcasted_iota(jnp.int32, (1, LANES), 1)
    live = lane < QK_DIM
    ones_lane = jnp.where(lane == VALUE_DIM, 1.0, 0.0).astype(F32)
    qu = jnp.dot(qu_ref[...], qe_ref[...], preferred_element_type=F32).astype(BF16)
    ku = jnp.dot(ku_ref[...], ke_ref[...], preferred_element_type=F32).astype(BF16)
    vu = jnp.dot(vu_ref[...], ve_ref[...], preferred_element_type=F32).astype(BF16)

    def tables(first_row, row_count, gain):
        gain_partner = pltpu.roll(gain, QK_DIM, 1)
        a = [(row_a[pl.ds(first_row + r, 1), :] + col_a[...]) * gain[0:1] for r in range(row_count)]
        b = [(row_b[pl.ds(first_row + r, 1), :] + col_b[...]) * gain_partner[0:1] for r in range(row_count)]
        return jnp.concatenate(a, axis=0), jnp.concatenate(b, axis=0)

    def finish(v, a, b):
        square = jnp.where(live, v * v, 0.0)
        factor = lax.rsqrt(jnp.sum(square, axis=-1, keepdims=True) * (1.0 / QK_DIM) + EPS)
        if b is None:
            return (v * a * factor).astype(BF16)
        return ((v * a + pltpu.roll(v, QK_DIM, 1) * b) * factor).astype(BF16)

    block = min(256, group)
    grid_rows = block // GRID_W
    qgain = qgain_ref[...]
    kgain = kgain_ref[...]

    def query_block(i, carry):
        start = pl.multiple_of(i * block, block)
        q = jnp.dot(q_ref[pl.ds(start, block), :], qu, preferred_element_type=F32)
        a, b = tables(s_ref[0] * (group // GRID_W) + i * grid_rows, grid_rows, qgain)
        for h in range(heads):
            q_all[h, pl.ds(start, block), :] = finish(q[:, h * LANES : (h + 1) * LANES], a, b)
        return carry

    lax.fori_loop(0, group // block, query_block, 0)

    def key_block(i, carry):
        start = pl.multiple_of(i * block, block)
        lat = kv_ref[pl.ds(start, block), :rank]
        rope = kv_ref[pl.ds(start, block), rank:].astype(F32)
        k = jnp.dot(lat, ku, preferred_element_type=F32)
        v = jnp.dot(lat, vu, preferred_element_type=F32)
        a, b = tables(i * grid_rows, grid_rows, kgain)
        for h in range(heads):
            k_lat[h, pl.ds(start, block), :] = finish(k[:, h * LANES : (h + 1) * LANES] + rope, a, b)
            v_lat[h, pl.ds(start, block), :] = (v[:, h * LANES : (h + 1) * LANES] + ones_lane).astype(BF16)
        return carry

    lax.fori_loop(0, tokens // block, key_block, 0)
    plain = jnp.where(live, kgain[0:1], 0.0)

    def context_block(i, carry):
        start = pl.multiple_of(i * block, block)
        lat = ctx_ref[pl.ds(start, block), :rank]
        rope = ctx_ref[pl.ds(start, block), rank:].astype(F32)
        k = jnp.dot(lat, ku, preferred_element_type=F32)
        v = jnp.dot(lat, vu, preferred_element_type=F32)
        for h in range(heads):
            k_ctx[h, pl.ds(start, block), :] = finish(k[:, h * LANES : (h + 1) * LANES] + rope, plain, None)
            v_ctx[h, pl.ds(start, block), :] = (v[:, h * LANES : (h + 1) * LANES] + ones_lane).astype(BF16)
        return carry

    lax.fori_loop(0, context // block, context_block, 0)

    factor = LOG2E * QK_DIM ** (-0.5)
    contract = (((1,), (1,)), ((), ()))
    q_rows = min(256, group)

    def attend(i, carry):
        start = pl.multiple_of(i * q_rows, q_rows)
        outs = []
        for h in range(heads):
            q = q_all[h, pl.ds(start, q_rows), :]
            s_lat = lax.dot_general(q, k_lat[h], contract, preferred_element_type=F32)
            s_ctx = lax.dot_general(q, k_ctx[h], contract, preferred_element_type=F32)
            lift = lift_ref[h] * LOG2E
            top = jnp.maximum(
                jnp.max(s_lat, axis=-1, keepdims=True) * factor,
                jnp.max(s_ctx, axis=-1, keepdims=True) * factor + lift,
            )
            p_lat = jnp.exp2(s_lat * factor - top).astype(BF16)
            p_ctx = jnp.exp2(s_ctx * factor - (top - lift)).astype(BF16)
            acc = jnp.dot(p_lat, v_lat[h], preferred_element_type=F32) + jnp.dot(
                p_ctx, v_ctx[h], preferred_element_type=F32
            )
            outs.append((acc[:, :VALUE_DIM] / acc[:, VALUE_DIM : VALUE_DIM + 1]).astype(BF16))
        out_ref[pl.ds(start, q_rows), :] = jnp.concatenate(outs, axis=1)
        return carry

    lax.fori_loop(0, group // q_rows, attend, 0)


def partner(tp, index, d):
    if tp & (tp - 1):
        return lax.rem(index + d, tp)
    result = 0 * index
    bit = 1
    while bit < tp:
        here = lax.rem(index // bit, 2)
        result = result + bit * (lax.rem(here + 1, 2) if d & bit else here)
        bit *= 2
    return result


def partners(tp, d):
    if tp & (tp - 1):
        return [(i, (i + d) % tp) for i in range(tp)]
    return [(i, i ^ d) for i in range(tp)]


def tail_kernel(tp, dp, att_ref, tokens_ref, gate_ref, own_w, *rest):
    shares = rest[: tp - 1]
    out_ref, held, swapped, send_sem, recv_sem, w_send, w_recv = rest[tp - 1 :]
    t_me = lax.axis_index("tp")
    d_me = lax.axis_index("dp")
    rows, width = out_ref.shape
    share = shares[0].shape[0]
    barrier = pltpu.get_barrier_semaphore()
    for d in range(1, tp):
        pl.semaphore_signal(barrier, inc=1, device_id={"tp": partner(tp, t_me, d)}, device_id_type=MESH)
    for e in range(1, dp):
        pl.semaphore_signal(barrier, inc=1, device_id={"dp": lax.rem(d_me + e, dp)}, device_id_type=MESH)
    pl.semaphore_wait(barrier, tp - 1 + dp - 1)
    copies = []
    for d in range(1, tp):
        dest = partner(tp, t_me, d)
        cp = pltpu.make_async_remote_copy(
            src_ref=att_ref.at[dest], dst_ref=held.at[d - 1],
            send_sem=send_sem.at[d - 1], recv_sem=recv_sem.at[d - 1],
            device_id={"tp": dest}, device_id_type=MESH,
        )
        cp.start()
        copies.append(cp)
    swaps = []
    for d in range(1, tp):
        for e in range(1, dp):
            i = (d - 1) * (dp - 1) + e - 1
            cp = pltpu.make_async_remote_copy(
                src_ref=shares[d - 1], dst_ref=swapped.at[i],
                send_sem=w_send.at[i], recv_sem=w_recv.at[i],
                device_id={"dp": lax.rem(d_me + e, dp)}, device_id_type=MESH,
            )
            cp.start()
            swaps.append(cp)
    chunk = 512
    spans = [slice(n * chunk, (n + 1) * chunk) for n in range(width // chunk)]
    mixed = [
        jnp.dot(att_ref[t_me], own_w[:, cols], preferred_element_type=F32).astype(BF16).astype(F32) for cols in spans
    ]
    for d in range(1, tp):
        copies[d - 1].wait()
        for e in range(1, dp):
            swaps[(d - 1) * (dp - 1) + e - 1].wait()
        parts = []
        for e in range(dp):
            owner = lax.rem(d_me + dp - e, dp)
            columns = pl.ds(pl.multiple_of(owner * share, share), share)
            parts.append(held[d - 1, :, columns])
        for n, cols in enumerate(spans):
            term = jnp.dot(parts[0], shares[d - 1][:, cols], preferred_element_type=F32)
            for e in range(1, dp):
                term = term + jnp.dot(
                    parts[e], swapped[(d - 1) * (dp - 1) + e - 1, :, cols], preferred_element_type=F32
                )
            mixed[n] = mixed[n] + term.astype(BF16).astype(F32)
    for n, cols in enumerate(spans):
        out_ref[:, cols] = (tokens_ref[:, cols].astype(F32) + gate_ref[:, cols] * mixed[n]).astype(BF16)


def local(
    sp, tp, dp,
    latent_tokens, condition, shift_weight, scale_weight, gate_weight, norm_gain,
    query_down, query_gain, kv_down, kv_gain, rope_down, query_up, key_up, value_up,
    query_norm_gain, key_norm_gain, out_weight, context_latent, context_rope, context_lift,
):
    rows, width = latent_tokens.shape
    q_rank = query_down.shape[1]
    rank = kv_down.shape[1]
    heads = query_up.shape[1] // QK_DIM
    ctx_rows = context_latent.shape[0]
    group = rows * tp
    tokens = group * sp
    n_dev = sp * tp

    front = pl.pallas_call(
        functools.partial(front_kernel, sp, tp),
        out_shape=(
            jax.ShapeDtypeStruct((tp, rows, q_rank), BF16),
            jax.ShapeDtypeStruct((n_dev, rows, rank + LANES), BF16),
            jax.ShapeDtypeStruct((sp, ctx_rows, rank + LANES), BF16),
            jax.ShapeDtypeStruct((1, width), F32),
        ),
        in_specs=[VMEM_SPEC] + [ANY_SPEC] * 4
        + [VMEM_SPEC, ANY_SPEC, VMEM_SPEC, ANY_SPEC, VMEM_SPEC, VMEM_SPEC, VMEM_SPEC, VMEM_SPEC, VMEM_SPEC],
        out_specs=(ANY_SPEC, ANY_SPEC, ANY_SPEC, VMEM_SPEC),
        scratch_shapes=[
            pltpu.VMEM((n_dev, 8, width // tp // 2), F32),
            pltpu.VMEM((rows, q_rank), BF16),
            pltpu.VMEM((rows, rank + LANES), BF16),
            pltpu.VMEM((ctx_rows, rank + LANES), BF16),
            pltpu.SemaphoreType.DMA((n_dev - 1,)),
            pltpu.SemaphoreType.DMA((n_dev - 1,)),
            pltpu.SemaphoreType.DMA((tp - 1,)),
            pltpu.SemaphoreType.DMA((tp - 1,)),
            pltpu.SemaphoreType.DMA((n_dev - 1,)),
            pltpu.SemaphoreType.DMA((n_dev - 1,)),
            pltpu.SemaphoreType.DMA((sp - 1,)),
            pltpu.SemaphoreType.DMA((sp - 1,)),
            pltpu.SemaphoreType.DMA((3,)),
            pltpu.VMEM(shift_weight.shape, BF16),
            pltpu.VMEM(scale_weight.shape, BF16),
            pltpu.VMEM(gate_weight.shape, BF16),
            pltpu.VMEM(latent_tokens.shape, BF16),
            pltpu.VMEM(query_down.shape, BF16),
            pltpu.VMEM(kv_down.shape, BF16),
            pltpu.SemaphoreType.DMA((6,)),
        ],
        compiler_params=pltpu.CompilerParams(
            collective_id=0, has_side_effects=True, vmem_limit_bytes=60 * 1024 * 1024
        ),
        cost_estimate=pl.CostEstimate(flops=20_000_000_000, bytes_accessed=8_000_000, transcendentals=0),
        name="front",
    )
    q_group, kv_all, ctx_all, mod_gate = front(
        condition[None], shift_weight, scale_weight, gate_weight, latent_tokens, norm_gain[None],
        query_down, query_gain[None], kv_down, kv_gain[None], rope_down.T,
        context_latent, context_rope.T, jnp.asarray(rope_spread(), BF16),
    )

    share = out_weight.shape[0] // dp
    mine, mod_gate = lax.optimization_barrier((
        lax.dynamic_slice_in_dim(out_weight, lax.axis_index("dp") * share, share, axis=0), mod_gate
    ))
    shares = [lax.ppermute(mine, "tp", partners(tp, d)) for d in range(1, tp)]

    def extended(gain):
        freq = ROPE_DIM // 4
        parts = [gain]
        for axis in range(2):
            start = NOPE_DIM + axis * 2 * freq
            parts += [gain[start + freq : start + 2 * freq], gain[start : start + freq]]
        return jnp.broadcast_to(jnp.concatenate(parts)[None], (8, LANES))

    row_a, row_b = turn_tables(tokens // GRID_W, 0)
    col_a, col_b = turn_tables(GRID_W, 1)
    context = sp * ctx_rows
    smem = pl.BlockSpec(memory_space=pltpu.SMEM)
    attended = pl.pallas_call(
        functools.partial(attend_kernel, heads),
        out_shape=jax.ShapeDtypeStruct((group, heads * VALUE_DIM), BF16),
        in_specs=[smem] + [VMEM_SPEC] * 11 + [smem] + [VMEM_SPEC] * 4,
        out_specs=VMEM_SPEC,
        scratch_shapes=[
            pltpu.VMEM((heads, tokens, LANES), BF16),
            pltpu.VMEM((heads, tokens, LANES), BF16),
            pltpu.VMEM((heads, context, LANES), BF16),
            pltpu.VMEM((heads, context, LANES), BF16),
            pltpu.VMEM((heads, group, LANES), BF16),
        ],
        compiler_params=pltpu.CompilerParams(vmem_limit_bytes=60 * 1024 * 1024),
        cost_estimate=pl.CostEstimate(flops=20_000_000_000, bytes_accessed=8_000_000, transcendentals=0),
        name="attend",
    )(
        lax.axis_index("sp").astype(jnp.int32)[None],
        q_group.reshape(group, q_rank), kv_all.reshape(tokens, rank + LANES),
        ctx_all.reshape(context, rank + LANES), query_up, key_up, value_up,
        jnp.asarray(query_spread(heads), BF16), jnp.asarray(head_spread(heads, NOPE_DIM), BF16),
        jnp.asarray(head_spread(heads, VALUE_DIM), BF16),
        extended(query_norm_gain), extended(key_norm_gain), context_lift,
        jnp.asarray(row_a), jnp.asarray(row_b), jnp.asarray(col_a), jnp.asarray(col_b),
    )

    return pl.pallas_call(
        functools.partial(tail_kernel, tp, dp),
        out_shape=jax.ShapeDtypeStruct((rows, width), BF16),
        in_specs=[VMEM_SPEC] * (3 + tp),
        out_specs=VMEM_SPEC,
        scratch_shapes=[
            pltpu.VMEM((tp - 1, rows, heads * VALUE_DIM), BF16),
            pltpu.VMEM(((tp - 1) * (dp - 1), share, width), BF16),
            pltpu.SemaphoreType.DMA((tp - 1,)),
            pltpu.SemaphoreType.DMA((tp - 1,)),
            pltpu.SemaphoreType.DMA(((tp - 1) * (dp - 1),)),
            pltpu.SemaphoreType.DMA(((tp - 1) * (dp - 1),)),
        ],
        compiler_params=pltpu.CompilerParams(
            collective_id=1, has_side_effects=True, vmem_limit_bytes=32 * 1024 * 1024
        ),
        name="tail",
    )(attended.reshape(tp, rows, heads * VALUE_DIM), latent_tokens, mod_gate, out_weight, *shares)


def solution(mesh):
    in_specs = (
        P(("dp", "sp", "tp"), None), P(("dp", "sp")), P("sp", "tp"), P("sp", "tp"), P("sp", "tp"),
        P(), P(), P(), P(), P(), P(), P(None, "tp"), P(None, "tp"), P(None, "tp"), P(), P(),
        P("tp", None), P(("dp", "sp"), None), P(("dp", "sp"), None), P("tp"),
    )
    out_specs = P(("dp", "sp", "tp"), None)
    body = functools.partial(local, mesh.shape["sp"], mesh.shape["tp"], mesh.shape["dp"])
    return jax.shard_map(body, mesh=mesh, in_specs=in_specs, out_specs=out_specs, check_vma=False)
```

profile of v0, /device:TPU:8, one launch (start us, length us, event | category | flops | bytes accessed | tf_op | source)
XLA Modules:
  0.0 103.7 jit_solution(15399790001666252602)
XLA Ops:
  0.0 1.3 %broadcast_in_dim.28.cond_ref = bf16[1,512]{1,0:T(2,128)(2,1)} reshape(bf16[512]{0:T(512)(128)(2,1)} %param.29) | data formatting | bytes 2048 | tf_op jit(solution)/shard_map/broadcast_in_dim | solution.py:437
  1.3 1.1 %constant_dynamic-slice_fusion = bf16[128,2048]{1,0:T(8,128)(2,1)S(1)} fusion(bf16[256,2048]{1,0:T(8,128)(2,1)} %own_w.1, s32[]{:T(128)S(6)} %select_n.3), kind=kLoop, calls=%fused_computation | loop fusion | bytes 1048580 | tf_op jit(solution)/shard_map/dynamic_slice | solution.py:444
  2.3 0.0 copy-start.4
  2.4 0.0 copy-start.5
  2.4 61.4 %front.1 = (bf16[4,128,512]{2,1,0:T(8,128)(2,1)}, bf16[16,128,384]{2,1,0:T(8,128)(2,1)}, bf16[4,256,384]{2,1,0:T(8,128)(2,1)}, f32[1,2048]{1,0:T(1,128)}) custom-call(bf16[1,512]{1,0:T(2,128)(2,1)} %broadcast_in_dim.28.cond_ref, bf16[512,512]{1,0:T(8,128)(2,1)} %shift_hbm.1, bf16[512,512]{1,0:T(8,128)(2,1)} %scale_hbm.1, bf16[512,512]{1,0:T(8,128)(2,1)} %gate_hbm.1, ...), custom_call_target="tpu_custom_call" | custom-call | flops 20000000000 | bytes 8000000 | tf_op jit(solution)/shard_map/front/pallas_call | solution.py:436
  63.7 1.6 %collective-permute-start = (bf16[128,2048]{1,0:T(8,128)(2,1)S(1)}, bf16[128,2048]{1,0:T(8,128)(2,1)S(1)}, u32[]{:S(2)}, u32[]{:S(2)}) collective-permute-start(bf16[128,2048]{1,0:T(8,128)(2,1)S(1)} %constant_dynamic-slice_fusion), channel_id=1, source_target_pairs={{0,2},{2,0},{4,6},{6,4},{1,3},{3,1},{5,7},{7,5},{8,10},{10,8},{12,... | collective-permute-start | bytes 1572872 | tf_op jit(solution)/shard_map/ppermute | solution.py:446
  65.3 1.4 %collective-permute-start.1 = (bf16[128,2048]{1,0:T(8,128)(2,1)S(1)}, bf16[128,2048]{1,0:T(8,128)(2,1)S(1)}, u32[]{:S(2)}, u32[]{:S(2)}) collective-permute-start(bf16[128,2048]{1,0:T(8,128)(2,1)S(1)} %constant_dynamic-slice_fusion), channel_id=1, source_target_pairs={{0,4},{2,6},{4,0},{6,2},{1,5},{3,7},{5,1},{7,3},{8,12},{10,14},{12... | collective-permute-start | bytes 1572872 | tf_op jit(solution)/shard_map/ppermute | solution.py:446
  66.7 0.6 collective-permute-start.2
  67.3 0.0 copy-done.4
  67.3 0.1 fusion.1
  67.4 0.0 copy-done.5
  67.4 0.1 fusion
  67.4 0.1 concatenate.6
  67.5 0.1 concatenate.7
  67.6 0.6 broadcast_in_dim.32.qgain_ref
  68.2 0.6 broadcast_in_dim.33.kgain_ref
  68.8 0.0 copy-start
  68.8 0.0 copy-start.1
  68.8 0.0 copy-start.3
  68.8 26.1 %attend.1 = bf16[512,256]{1,0:T(8,128)(2,1)} custom-call(s32[1]{0:T(128)} %bitcast.s_ref, bf16[512,512]{1,0:T(8,128)(2,1)} %bitcast.18, bf16[2048,384]{1,0:T(8,128)(2,1)} %bitcast.16, bf16[1024,384]{1,0:T(8,128)(2,1)} %bitcast.17, bf16[512,384]{1,0:T(8,128)(2,1)} %qu_ref.1, bf16[256,256]{1,0:T(8,128)(2,1)} %ku_ref.1, bf16[256,256]{1,0:T(8,128)(2,1)} %vu_ref.1, ...), custom_call_target="tpu_custom_call" | custom-call | flops 20000000000 | bytes 8000000 | tf_op jit(solution)/shard_map/attend/pallas_call | solution.py:460
  94.8 0.0 collective-permute-done.rest_0_
  94.8 0.0 collective-permute-done.1.rest_1_
  94.8 0.0 collective-permute-done.2.rest_2_
  94.9 0.0 copy-done
  94.9 0.0 copy-done.1
  94.9 0.0 copy-done.3
  94.9 0.0 copy-start.2
  94.9 0.9 copy-done.2
  95.8 7.1 %tail.1 = bf16[128,2048]{1,0:T(8,128)(2,1)S(1)} custom-call(bf16[4,128,256]{2,1,0:T(8,128)(2,1)S(1)} %bitcast.10, bf16[128,2048]{1,0:T(8,128)(2,1)S(1)} %copy-done.1, f32[1,2048]{1,0:T(1,128)S(1)} %copy-done.3, bf16[256,2048]{1,0:T(8,128)(2,1)S(1)} %copy-done, bf16[128,2048]{1,0:T(8,128)(2,1)S(1)} %collective-permute-done.rest_0_, ...), custom_call_target="tpu_custom_call" | custom-call | tf_op jit(solution)/shard_map/tail/pallas_call | solution.py:485
  102.9 0.8 copy.30
Async XLA Ops:
  2.3 64.9 %copy-start.4 = (f32[96]{0:T(128)S(1)}, f32[96]{0:T(128)}, u32[]{:S(2)}) copy-start(f32[96]{0:T(128)} %param.42) | copy-start | bytes 1156
  2.4 65.0 %copy-start.5 = (f32[96]{0:T(128)S(1)}, f32[96]{0:T(128)}, u32[]{:S(2)}) copy-start(f32[96]{0:T(128)} %param.43) | copy-start | bytes 1156
  63.7 31.1 %collective-permute-start = (bf16[128,2048]{1,0:T(8,128)(2,1)S(1)}, bf16[128,2048]{1,0:T(8,128)(2,1)S(1)}, u32[]{:S(2)}, u32[]{:S(2)}) collective-permute-start(bf16[128,2048]{1,0:T(8,128)(2,1)S(1)} %constant_dynamic-slice_fusion), channel_id=1, source_target_pairs={{0,2},{2,0},{4,6},{6,4},{1,3},{3,1},{5,7},{7,5},{8,10},{10,8},{12,... | collective-permute-start | bytes 1572872 | tf_op jit(solution)/shard_map/ppermute | solution.py:446
  65.3 29.6 %collective-permute-start.1 = (bf16[128,2048]{1,0:T(8,128)(2,1)S(1)}, bf16[128,2048]{1,0:T(8,128)(2,1)S(1)}, u32[]{:S(2)}, u32[]{:S(2)}) collective-permute-start(bf16[128,2048]{1,0:T(8,128)(2,1)S(1)} %constant_dynamic-slice_fusion), channel_id=1, source_target_pairs={{0,4},{2,6},{4,0},{6,2},{1,5},{3,7},{5,1},{7,3},{8,12},{10,14},{12... | collective-permute-start | bytes 1572872 | tf_op jit(solution)/shard_map/ppermute | solution.py:446
  66.7 28.1 %collective-permute-start.2 = (bf16[128,2048]{1,0:T(8,128)(2,1)S(1)}, bf16[128,2048]{1,0:T(8,128)(2,1)S(1)}, u32[]{:S(2)}, u32[]{:S(2)}) collective-permute-start(bf16[128,2048]{1,0:T(8,128)(2,1)S(1)} %constant_dynamic-slice_fusion), channel_id=1, source_target_pairs={{0,6},{2,4},{4,2},{6,0},{1,7},{3,5},{5,3},{7,1},{8,14},{10,12},{12... | collective-permute-start | bytes 1572872 | tf_op jit(solution)/shard_map/ppermute | solution.py:446
  68.8 26.1 %copy-start = (bf16[256,2048]{1,0:T(8,128)(2,1)S(1)}, bf16[256,2048]{1,0:T(8,128)(2,1)}, u32[]{:S(2)}) copy-start(bf16[256,2048]{1,0:T(8,128)(2,1)} %own_w.1) | copy-start | bytes 3145732
  68.8 26.1 %copy-start.1 = (bf16[128,2048]{1,0:T(8,128)(2,1)S(1)}, bf16[128,2048]{1,0:T(8,128)(2,1)}, u32[]{:S(2)}) copy-start(bf16[128,2048]{1,0:T(8,128)(2,1)} %tokens_ref.1) | copy-start | bytes 1572868
  68.8 26.1 %copy-start.3 = (f32[1,2048]{1,0:T(1,128)S(1)}, f32[1,2048]{1,0:T(1,128)}, u32[]{:S(2)}) copy-start(f32[1,2048]{1,0:T(1,128)} %get-tuple-element.15.gate_ref) | copy-start | bytes 24580
  94.9 1.0 copy-start.2
where the time goes:
time: 104 us
  Pallas kernels  94.5 us (91%)
  local copies, waits for them, and re-layouts  5.58 us (5%)
  starting transfers between devices  3.55 us (3%)
    pallas_call x1, Pallas kernels, local(): front(condition[None], shift_weight, scale_weight, gate_weight, latent_to...  61.4 us
    pallas_call x1, Pallas kernels, local(): pl.pallas_call(functools.partial(attend_kernel, heads), out_shape=jax.Sha...  26.1 us
    pallas_call x1, Pallas kernels, local(): pl.pallas_call(functools.partial(tail_kernel, tp, dp), out_shape=jax.Shap...  7.08 us
    ppermute x3, starting transfers between devices, local(): shares = [lax.ppermute(mine, 'tp', partners(tp, d)) for d in range(1, tp)]  3.55 us
  transfers between devices with their start and end apart: 3, of which 0 were waited for; matrix products, arithmetic and copies ran while one was open for 1% of the time, Pallas kernels for 25%

commit v1 on v0

v1 whole, which is shorter than its diff:
```python
import functools

import jax
import jax.numpy as jnp
import numpy as np
from jax import lax
from jax.experimental import pallas as pl
from jax.experimental.pallas import tpu as pltpu
from jax.sharding import PartitionSpec as P

NOPE_DIM = 64
ROPE_DIM = 32
VALUE_DIM = 64
QK_DIM = 96
GRID_W = 64
LANES = 128

EPS = 1e-06
THETA = 10000.0
LOG2E = 1.4426950408889634
MESH = pl.DeviceIdType.MESH
VMEM_SPEC = pl.BlockSpec(memory_space=pltpu.VMEM)
ANY_SPEC = pl.BlockSpec(memory_space=pl.ANY)
BF16 = jnp.bfloat16
F32 = jnp.float32


def partner_order():
    return np.arange(ROPE_DIM) ^ (ROPE_DIM // 4)


def rope_spread():
    spread = np.zeros((ROPE_DIM, LANES), np.float32)
    order = partner_order()
    for j in range(ROPE_DIM):
        spread[j, NOPE_DIM + j] = 1.0
        spread[order[j], QK_DIM + j] = 1.0
    return spread


def query_spread(heads):
    spread = np.zeros((heads * QK_DIM, heads * LANES), np.float32)
    order = partner_order()
    for h in range(heads):
        for j in range(QK_DIM):
            spread[h * QK_DIM + j, h * LANES + j] = 1.0
        for j in range(ROPE_DIM):
            spread[h * QK_DIM + NOPE_DIM + order[j], h * LANES + QK_DIM + j] = 1.0
    return spread


def head_spread(heads, width):
    spread = np.zeros((heads * width, heads * LANES), np.float32)
    for h in range(heads):
        for j in range(width):
            spread[h * width + j, h * LANES + j] = 1.0
    return spread


def turn_tables(count, axis):
    freq_count = ROPE_DIM // 4
    inverse = np.float32(THETA) ** (-np.float32(4.0) * np.arange(freq_count, dtype=np.float32) / np.float32(ROPE_DIM))
    angles = np.arange(count, dtype=np.float32)[:, None] * inverse.astype(np.float32)
    cosine = np.zeros((count, LANES), np.float32)
    sine = np.zeros((count, LANES), np.float32)
    start = NOPE_DIM + axis * 2 * freq_count
    mid = start + freq_count
    cosine[:, start:mid] = np.cos(angles.astype(np.float64))
    cosine[:, mid : mid + freq_count] = np.cos(angles.astype(np.float64))
    sine[:, start:mid] = -np.sin(angles.astype(np.float64))
    sine[:, mid : mid + freq_count] = np.sin(angles.astype(np.float64))
    if axis == 0:
        cosine[:, :NOPE_DIM] = 1.0
    return cosine, sine


def norm_factor(values):
    return lax.rsqrt(jnp.mean(values * values, axis=-1, keepdims=True) + EPS)


def partner(tp, index, d):
    if tp & (tp - 1):
        return lax.rem(index + d, tp)
    result = 0 * index
    bit = 1
    while bit < tp:
        here = lax.rem(index // bit, 2)
        result = result + bit * (lax.rem(here + 1, 2) if d & bit else here)
        bit *= 2
    return result


def fused_kernel(
    sp, tp, dp, heads,
    cond_ref, gain_ref, qg_ref, kg_ref, qgain_ref, kgain_ref, lift_ref, row_a, row_b, col_a, col_b, spread_ref,
    shift_hbm, scale_hbm, gate_hbm, tokens_hbm, qd_hbm, kd_hbm, rd_hbm, cl_hbm, cr_hbm,
    qu_hbm, ku_hbm, vu_hbm, qe_hbm, ke_hbm, ve_hbm, w_hbm,
    out_ref,
    mods, q_lat, kv, ctx, ctx_rope, gate_buf, tab_a, tab_b, gains, q_all, k_buf, v_buf, k_ctx, v_ctx, top_ref, acc_ref, att, held,
    w_all, shift_w, scale_w, gate_w, tokens_ref, qd_ref, kd_ref, rd_ref,
    qu_raw, ku_raw, vu_raw, qe_ref, ke_ref, ve_ref, qu_ref, ku_ref, vu_ref,
    load_sem, mod_send, mod_recv, q_send, q_recv, kv_send, kv_recv, c_send, c_recv, w_send, w_recv,
    x_send, x_recv, a_send, a_recv,
):
    s_me = lax.axis_index("sp")
    t_me = lax.axis_index("tp")
    d_me = lax.axis_index("dp")
    me = s_me * tp + t_me
    half = mods.shape[2]
    rows = tokens_ref.shape[0]
    rank = ku_raw.shape[0]
    group = tp * rows
    ctx_rows = cl_hbm.shape[0]
    share = w_hbm.shape[0] // dp
    width = w_hbm.shape[1]
    pieces = rank // rows

    def load(i, src, dst):
        cp = pltpu.make_async_copy(src, dst, load_sem.at[i])
        cp.start()
        return cp

    first = [
        load(i, src, dst)
        for i, (src, dst) in enumerate(((shift_hbm, shift_w), (scale_hbm, scale_w), (gate_hbm, gate_w)))
    ]
    ctx_load = [
        load(3, cl_hbm, ctx.at[0]),
        load(4, cr_hbm, ctx_rope.at[0]),
    ]
    w_load = load(5, w_hbm, w_all.at[0])
    token_load = load(6, tokens_hbm, tokens_ref)
    down_load = [load(7, qd_hbm, qd_ref), load(8, kd_hbm, kd_ref), load(9, rd_hbm, rd_ref)]
    up_load = [
        load(10 + i, src, dst)
        for i, (src, dst) in enumerate((
            (qu_hbm, qu_raw), (ku_hbm, ku_raw), (vu_hbm, vu_raw), (qe_hbm, qe_ref), (ke_hbm, ke_ref), (ve_hbm, ve_ref),
        ))
    ]

    def peer(ds, dt):
        return {"sp": lax.rem(s_me + ds, sp), "tp": lax.rem(t_me + dt, tp)}

    def column(ds):
        return {"sp": lax.rem(s_me + ds, sp)}

    def mate(d):
        return {"tp": partner(tp, t_me, d)}

    def twin(e):
        return {"dp": lax.rem(d_me + e, dp)}

    def remote(src, dst, send, recv, device):
        return pltpu.make_async_remote_copy(
            src_ref=src, dst_ref=dst, send_sem=send, recv_sem=recv, device_id=device, device_id_type=MESH
        )

    others = [(ds, dt) for ds in range(sp) for dt in range(tp) if ds or dt]
    barrier = pltpu.get_barrier_semaphore()
    for ds, dt in others:
        pl.semaphore_signal(barrier, inc=1, device_id=peer(ds, dt), device_id_type=MESH)
    for e in range(1, dp):
        pl.semaphore_signal(barrier, inc=1, device_id=twin(e), device_id_type=MESH)

    with jax.named_scope("modmm"):
        c = cond_ref[...].astype(F32)
        act = (c / (1.0 + jnp.exp(-c))).astype(BF16)
        act = jnp.broadcast_to(act, (16, act.shape[1]))
        terms = []
        for i, w in enumerate((shift_w, scale_w, gate_w)):
            first[i].wait()
            term = jnp.dot(act, w[...], preferred_element_type=F32)[0:1]
            terms += [term[:, :half], term[:, half:]]
        mods[me] = jnp.concatenate(terms + [terms[0], terms[0]], axis=0)
        for cp in ctx_load:
            cp.wait()
        w_load.wait()

    with jax.named_scope("barrier"):
        pl.semaphore_wait(barrier, len(others) + dp - 1)
    mod_copies = []
    for i, (ds, dt) in enumerate(others):
        mod_copies.append(remote(mods.at[me], mods.at[me], mod_send.at[i], mod_recv.at[i], peer(ds, dt)))
        mod_copies[-1].start()
    ctx_copies = []
    for ds in range(1, sp):
        for k, buf in enumerate((ctx, ctx_rope)):
            i = 2 * ds - 2 + k
            ctx_copies.append(remote(buf.at[0], buf.at[ds], c_send.at[i], c_recv.at[i], column(ds)))
            ctx_copies[-1].start()

    cut = share // 2
    my_start = pl.multiple_of(d_me * share, share)

    def w_copy(d, part):
        span = pl.ds(pl.multiple_of(my_start + part * cut, cut), cut)
        i = (d - 1) * 2 + part
        return remote(w_all.at[0, span], w_all.at[d, span], w_send.at[i], w_recv.at[i], mate(d))

    early = [(d, 0) for d in range(1, tp - 1)]
    late = [(d, part) for d in range(1, tp) for part in range(2) if (d, part) not in early]
    for d, part in early:
        w_copy(d, part).start()

    with jax.named_scope("prep"):
        gains[...] = jnp.zeros(gains.shape, F32)
        gains[0:1, :QK_DIM] = qgain_ref[...]
        gains[1:2, :QK_DIM] = kgain_ref[...]
        lane = lax.broadcasted_iota(jnp.int32, (1, LANES), 1)
        freq = ROPE_DIM // 4
        low = lax.rem(lane, 2 * freq) < freq
        live = lane < QK_DIM
        ones_lane = jnp.where(lane == VALUE_DIM, 1.0, 0.0).astype(F32)
        qgain = gains[0:1, :]
        kgain = gains[1:2, :]

        def swap(g):
            return jnp.where(low, pltpu.roll(g, LANES - freq, 1), pltpu.roll(g, freq, 1))

        qgain_swap = swap(qgain)
        kgain_swap = swap(kgain)

        def fill_tables(r, carry):
            span = pl.ds(pl.multiple_of(r * GRID_W, GRID_W), GRID_W)
            tab_a[span, :] = row_a[pl.ds(r, 1), :] + col_a[...]
            tab_b[span, :] = row_b[pl.ds(r, 1), :] + col_b[...]
            return carry

        lax.fori_loop(0, tab_a.shape[0] // GRID_W, fill_tables, 0)
        for cp in up_load:
            cp.wait()
        factor = LOG2E * QK_DIM ** (-0.5)
        qu_ref[...] = jnp.dot(qu_raw[...], qe_ref[...], preferred_element_type=F32).astype(BF16)
        ku_ref[...] = jnp.dot(ku_raw[...], ke_ref[...], preferred_element_type=F32).astype(BF16)
        vu_ref[...] = jnp.dot(vu_raw[...], ve_ref[...], preferred_element_type=F32).astype(BF16)
        spread = spread_ref[...]
        token_load.wait()
        for cp in down_load:
            cp.wait()
        x = tokens_ref[...].astype(F32)
        xn = x * norm_factor(x) * gain_ref[...]

    with jax.named_scope("waitmods"):
        for cp in mod_copies:
            cp.wait_recv()
    with jax.named_scope("stageB"):
        parts = [[], [], []]
        for t in range(tp):
            total = mods[t]
            for s in range(1, sp):
                total = total + mods[s * tp + t]
            for k in range(3):
                parts[k] += [total[2 * k : 2 * k + 1], total[2 * k + 1 : 2 * k + 2]]
        shift, scale, gate = [jnp.concatenate(p, axis=1) for p in parts]
        gate_buf[...] = gate
        normed = (xn * (1.0 + scale) + shift).astype(BF16)
        q = jnp.dot(normed, qd_ref[...], preferred_element_type=F32)
        q_lat[0] = (q * norm_factor(q) * qg_ref[...]).astype(BF16)
        lat = jnp.dot(normed, kd_ref[...], preferred_element_type=F32)
        kv[0, 0, :rows, :] = (lat * norm_factor(lat) * kg_ref[...]).astype(BF16)
        rope = lax.dot_general(
            rd_ref[...], normed, (((1,), (1,)), ((), ())), preferred_element_type=F32
        ).astype(BF16)
        piece = ROPE_DIM // pieces
        for p in range(pieces):
            kv[0, 0, rows:, p * rows : (p + 1) * rows] = rope[p * piece : (p + 1) * piece]

    def q_copy(d):
        return remote(q_lat.at[0], q_lat.at[d], q_send.at[d - 1], q_recv.at[d - 1], mate(d))

    def kv_column(ds):
        return remote(kv.at[0, 0], kv.at[ds, 0], kv_send.at[ds, 0], kv_recv.at[ds, 0], column(ds))

    def kv_mate(ds, d):
        return remote(kv.at[ds, 0], kv.at[ds, d], kv_send.at[ds, d], kv_recv.at[ds, d], mate(d))

    for d in range(1, tp):
        q_copy(d).start()
    for ds in range(1, sp):
        kv_column(ds).start()
    for d in range(1, tp):
        kv_mate(0, d).start()

    contract = (((1,), (1,)), ((), ()))

    def expand(lat, rope_t, a, b, store):
        rope = lax.dot_general(rope_t, spread, (((0,), (0,)), ((), ())), preferred_element_type=F32)
        rope_square = jnp.sum(jnp.where(live, rope * rope, 0.0), axis=-1, keepdims=True)
        turned = rope * a if b is None else rope * a + pltpu.roll(rope, QK_DIM, 1) * b
        k = jnp.dot(lat, ku_ref[...], preferred_element_type=F32)
        v = jnp.dot(lat, vu_ref[...], preferred_element_type=F32)
        for h in range(heads):
            cols = slice(h * LANES, (h + 1) * LANES)
            kh = k[:, cols]
            square = jnp.sum(kh * kh, axis=-1, keepdims=True) + rope_square
            scale_h = lax.rsqrt(square * (1.0 / QK_DIM) + EPS)
            store(h, ((kh * kgain + turned) * scale_h).astype(BF16), (v[:, cols] + ones_lane).astype(BF16))

    def attend(start, count, keys, values, h, lift, fresh):
        span = pl.ds(start, count)
        s = lax.dot_general(q_all[h, span, :], keys, contract, preferred_element_type=F32)
        peak = jnp.max(s, axis=-1, keepdims=True)
        if lift is not None:
            peak = peak + lift
        if fresh:
            top = jnp.broadcast_to(peak, (count, LANES))
        else:
            old = top_ref[h, span, :]
            top = jnp.maximum(old, peak)
        top_ref[h, span, :] = top
        floor = top if lift is None else top - lift
        p = jnp.exp2(s - jnp.concatenate([floor] * (keys.shape[0] // LANES), axis=1)).astype(BF16)
        add = jnp.dot(p, values, preferred_element_type=F32)
        if not fresh:
            add = acc_ref[h, span, :] * jnp.exp2(old - top) + add
        acc_ref[h, span, :] = add

    with jax.named_scope("ctxwait"):
        for cp in ctx_copies:
            cp.wait_recv()
    with jax.named_scope("ctxexpand"):
        def context_block(i, carry):
            lat = ctx[i]
            rope_t = ctx_rope[i]

            def store(h, k, v):
                span = pl.ds(pl.multiple_of(i * ctx_rows, ctx_rows), ctx_rows)
                k_ctx[h, span, :] = k
                v_ctx[h, span, :] = v

            expand(lat, rope_t, kgain, None, store)
            return carry

        lax.fori_loop(0, sp, context_block, 0)

    for d in range(tp):
        slot = (tp - 1 - d) * rows
        with jax.named_scope("qwait"):
            if d:
                q_copy(d).wait_recv()
        with jax.named_scope("qctx"):
            start = pl.multiple_of((s_me * tp + (partner(tp, t_me, d) if d else t_me)) * rows, rows)
            a = tab_a[pl.ds(start, rows), :] * qgain
            b = tab_b[pl.ds(start, rows), :] * qgain_swap
            qx = jnp.dot(q_lat[d], qu_ref[...], preferred_element_type=F32)
            for h in range(heads):
                v = qx[:, h * LANES : (h + 1) * LANES]
                square = jnp.sum(jnp.where(live, v * v, 0.0), axis=-1, keepdims=True)
                scale_h = lax.rsqrt(square * (1.0 / QK_DIM) + EPS) * factor
                q_all[h, slot : slot + rows, :] = ((v * a + pltpu.roll(v, QK_DIM, 1) * b) * scale_h).astype(BF16)
            for h in range(heads):
                attend(slot, rows, k_ctx[h], v_ctx[h], h, lift_ref[h] * LOG2E, True)

    with jax.named_scope("zwait"):
        for ds in range(1, sp):
            kv_column(ds).wait_recv()
            for d in range(1, tp):
                kv_mate(ds, d).start()
    for d, part in late:
        w_copy(d, part).start()

    def x_copy(d, e):
        i = (d - 1) * (dp - 1) + e - 1
        span = pl.ds(my_start, share)
        return remote(w_all.at[d, span], w_all.at[d, span], x_send.at[i], x_recv.at[i], twin(e))

    q_rows = 2 * rows if tp % 2 == 0 else rows

    def group_step(i, carry):
        ds = lax.rem(lax.rem(i, 2) * ((i + 1) // 2) + lax.rem(i + 1, 2) * (sp - i // 2), sp)
        source = lax.rem(s_me + sp - ds, sp)
        with jax.named_scope("kvwait"):
            for d in range(1, tp):
                kv_mate(ds, d).wait_recv()
        with jax.named_scope("kvexpand"):
            for d in range(tp):
                start = pl.multiple_of((source * tp + (partner(tp, t_me, d) if d else t_me)) * rows, rows)
                a = tab_a[pl.ds(start, rows), :] * kgain
                b = tab_b[pl.ds(start, rows), :] * kgain_swap
                lat = kv[ds, d, pl.ds(0, rows), :]
                tail = kv[ds, d, pl.ds(rows, ROPE_DIM // pieces), :]
                rope_t = jnp.concatenate([tail[:, p * rows : (p + 1) * rows] for p in range(pieces)], axis=0)

                def store(h, k, v):
                    k_buf[h, d * rows : (d + 1) * rows, :] = k
                    v_buf[h, d * rows : (d + 1) * rows, :] = v

                expand(lat, rope_t, a, b, store)

        with jax.named_scope("attend"):

            def rows_step(j, inner):
                start = pl.multiple_of(j * q_rows, q_rows)
                for h in range(heads):
                    attend(start, q_rows, k_buf[h], v_buf[h], h, None, False)
                return inner

            lax.fori_loop(0, group // q_rows, rows_step, 0)

        @pl.when(i == sp - 2)
        def _():
            with jax.named_scope("wswap"):
                for d in range(1, tp):
                    for part in range(2):
                        w_copy(d, part).wait_recv()
                    for e in range(1, dp):
                        x_copy(d, e).start()

        return carry

    lax.fori_loop(0, sp, group_step, 0)

    def a_copy(d):
        return remote(att.at[d], held.at[d - 1], a_send.at[d - 1], a_recv.at[d - 1], mate(d))

    with jax.named_scope("finish"):
        for d in range(tp - 1, -1, -1):
            slot = (tp - 1 - d) * rows
            outs = []
            for h in range(heads):
                total = acc_ref[h, slot : slot + rows, :]
                outs.append((total[:, :VALUE_DIM] / total[:, VALUE_DIM : VALUE_DIM + 1]).astype(BF16))
            att[d] = jnp.concatenate(outs, axis=1)
            if d:
                a_copy(d).start()

    with jax.named_scope("tail"):
        chunk = 512
        spans = [slice(n * chunk, (n + 1) * chunk) for n in range(width // chunk)]
        mixed = [
            jnp.dot(att[0], w_all[0, :, cols], preferred_element_type=F32).astype(BF16).astype(F32) for cols in spans
        ]
        for d in range(1, tp):
            with jax.named_scope("xwait"):
                for e in range(1, dp):
                    x_copy(d, e).wait_recv()
            with jax.named_scope("await"):
                a_copy(d).wait_recv()
            for n, cols in enumerate(spans):
                term = jnp.dot(held[d - 1], w_all[d, :, cols], preferred_element_type=F32)
                mixed[n] = mixed[n] + term.astype(BF16).astype(F32)
        for n, cols in enumerate(spans):
            out_ref[:, cols] = (tokens_ref[:, cols].astype(F32) + gate_buf[:, cols] * mixed[n]).astype(BF16)

    with jax.named_scope("drain"):
        for cp in mod_copies + ctx_copies:
            cp.wait_send()
        for d in range(1, tp):
            q_copy(d).wait_send()
            a_copy(d).wait_send()
            for part in range(2):
                w_copy(d, part).wait_send()
            for e in range(1, dp):
                x_copy(d, e).wait_send()
            for ds in range(sp):
                kv_mate(ds, d).wait_send()
        for ds in range(1, sp):
            kv_column(ds).wait_send()


def local(
    sp, tp, dp,
    latent_tokens, condition, shift_weight, scale_weight, gate_weight, norm_gain,
    query_down, query_gain, kv_down, kv_gain, rope_down, query_up, key_up, value_up,
    query_norm_gain, key_norm_gain, out_weight, context_latent, context_rope, context_lift,
):
    rows, width = latent_tokens.shape
    q_rank = query_down.shape[1]
    rank = kv_down.shape[1]
    heads = query_up.shape[1] // QK_DIM
    ctx_rows = context_latent.shape[0]
    group = rows * tp
    tokens = group * sp
    context = sp * ctx_rows
    n_dev = sp * tp
    row_a, row_b = turn_tables(tokens // GRID_W, 0)
    col_a, col_b = turn_tables(GRID_W, 1)
    q_spread = jnp.asarray(query_spread(heads), BF16)
    k_spread = jnp.asarray(head_spread(heads, NOPE_DIM), BF16)
    v_spread = jnp.asarray(head_spread(heads, VALUE_DIM), BF16)
    dma = pltpu.SemaphoreType.DMA
    vmem = pltpu.VMEM
    return pl.pallas_call(
        functools.partial(fused_kernel, sp, tp, dp, heads),
        out_shape=jax.ShapeDtypeStruct((rows, width), BF16),
        in_specs=[VMEM_SPEC] * 6 + [pl.BlockSpec(memory_space=pltpu.SMEM)] + [VMEM_SPEC] * 5 + [ANY_SPEC] * 16,
        out_specs=VMEM_SPEC,
        scratch_shapes=[
            vmem((n_dev, 8, width // tp // 2), F32),
            vmem((tp, rows, q_rank), BF16),
            vmem((sp, tp, rows + ROPE_DIM * rows // rank, rank), BF16),
            vmem((sp, ctx_rows, rank), BF16),
            vmem((sp, ROPE_DIM, ctx_rows), BF16),
            vmem((1, width), F32),
            vmem((tokens, LANES), F32),
            vmem((tokens, LANES), F32),
            vmem((8, LANES), F32),
            vmem((heads, group, LANES), BF16),
            vmem((heads, group, LANES), BF16),
            vmem((heads, group, LANES), BF16),
            vmem((heads, context, LANES), BF16),
            vmem((heads, context, LANES), BF16),
            vmem((heads, group, LANES), F32),
            vmem((heads, group, LANES), F32),
            vmem((tp, rows, heads * VALUE_DIM), BF16),
            vmem((tp - 1, rows, heads * VALUE_DIM), BF16),
            vmem((tp,) + out_weight.shape, BF16),
            vmem(shift_weight.shape, BF16),
            vmem(scale_weight.shape, BF16),
            vmem(gate_weight.shape, BF16),
            vmem(latent_tokens.shape, BF16),
            vmem(query_down.shape, BF16),
            vmem(kv_down.shape, BF16),
            vmem(rope_down.shape[::-1], BF16),
            vmem(query_up.shape, BF16),
            vmem(key_up.shape, BF16),
            vmem(value_up.shape, BF16),
            vmem(q_spread.shape, BF16),
            vmem(k_spread.shape, BF16),
            vmem(v_spread.shape, BF16),
            vmem((q_rank, heads * LANES), BF16),
            vmem((rank, heads * LANES), BF16),
            vmem((rank, heads * LANES), BF16),
            dma((16,)),
            dma((n_dev - 1,)), dma((n_dev - 1,)),
            dma((tp - 1,)), dma((tp - 1,)),
            dma((sp, tp)), dma((sp, tp)),
            dma((2 * (sp - 1),)), dma((2 * (sp - 1),)),
            dma((2 * (tp - 1),)), dma((2 * (tp - 1),)),
            dma(((tp - 1) * (dp - 1),)), dma(((tp - 1) * (dp - 1),)),
            dma((tp - 1,)), dma((tp - 1,)),
        ],
        compiler_params=pltpu.CompilerParams(
            collective_id=0, has_side_effects=True, vmem_limit_bytes=60 * 1024 * 1024
        ),
        name="fused",
    )(
        condition[None], norm_gain[None], query_gain[None], kv_gain[None], query_norm_gain[None], key_norm_gain[None],
        context_lift, jnp.asarray(row_a), jnp.asarray(row_b), jnp.asarray(col_a), jnp.asarray(col_b),
        jnp.asarray(rope_spread(), BF16),
        shift_weight, scale_weight, gate_weight, latent_tokens, query_down, kv_down, rope_down.T,
        context_latent, context_rope.T, query_up, key_up, value_up, q_spread, k_spread, v_spread, out_weight,
    )


def solution(mesh):
    in_specs = (
        P(("dp", "sp", "tp"), None), P(("dp", "sp")), P("sp", "tp"), P("sp", "tp"), P("sp", "tp"),
        P(), P(), P(), P(), P(), P(), P(None, "tp"), P(None, "tp"), P(None, "tp"), P(), P(),
        P("tp", None), P(("dp", "sp"), None), P(("dp", "sp"), None), P("tp"),
    )
    out_specs = P(("dp", "sp", "tp"), None)
    body = functools.partial(local, mesh.shape["sp"], mesh.shape["tp"], mesh.shape["dp"])
    return jax.shard_map(body, mesh=mesh, in_specs=in_specs, out_specs=out_specs, check_vma=False)
```

time: 104 us -> 77.1 us (0.74)
  the two profiles are of different devices: /device:TPU:8 before, /device:TPU:0 now
where the time goes in v1:
time: 77.1 us; the launch traced here: 76.5 us
  Pallas kernels  73.3 us (95%)
  local copies, waits for them, and re-layouts  3.14 us (4%)
    pallas_call x1, Pallas kernels, local(): pl.pallas_call(functools.partial(fused_kernel, sp, tp, dp, heads), out_sh...  73.3 us
    unnamed x1, local copies, waits for them, and re-layouts  1.88 us

profile of v1, /device:TPU:0, one launch (start us, length us, event | category | flops | bytes accessed | tf_op | source)
XLA Modules:
  0.0 76.5 jit_solution(17157677420248094923)
XLA Ops:
  0.0 1.3 %broadcast_in_dim.18.cond_ref = bf16[1,512]{1,0:T(2,128)(2,1)} reshape(bf16[512]{0:T(512)(128)(2,1)} %param.29) | data formatting | bytes 2048 | tf_op jit(solution)/shard_map/broadcast_in_dim | solution.py:538
  1.3 73.3 %fused.1 = bf16[128,2048]{1,0:T(8,128)(2,1)} custom-call(bf16[1,512]{1,0:T(2,128)(2,1)} %broadcast_in_dim.18.cond_ref, f32[1,2048]{1,0:T(1,128)} %bitcast.9, f32[1,512]{1,0:T(1,128)} %bitcast.10, f32[1,256]{1,0:T(1,128)} %bitcast.11, f32[1,96]{1,0:T(1,128)} %bitcast.12, f32[1,96]{1,0:T(1,128)} %bitcast.13, f32[4]{0:T(128)} %lift_ref.1, ...), custom_call_target="tpu_custom_call" | custom-call | tf_op jit(solution)/shard_map/fused/pallas_call | solution.py:483
  74.6 1.9 %copy.30 = bf16[128,2048]{1,0:T(8,128)(2,1)} copy(bf16[128,2048]{1,0:T(8,128)(2,1)} %fused.1) | data formatting | bytes 1048576

commit v2 on v1

--- a/solution.py
+++ b/solution.py
@@ -20,7 +20,7 @@
 LOG2E = 1.4426950408889634
 MESH = pl.DeviceIdType.MESH
 VMEM_SPEC = pl.BlockSpec(memory_space=pltpu.VMEM)
-ANY_SPEC = pl.BlockSpec(memory_space=pl.ANY)
+HBM_SPEC = pl.BlockSpec(memory_space=pltpu.HBM)
 BF16 = jnp.bfloat16
 F32 = jnp.float32
 
@@ -96,22 +96,23 @@
     shift_hbm, scale_hbm, gate_hbm, tokens_hbm, qd_hbm, kd_hbm, rd_hbm, cl_hbm, cr_hbm,
     qu_hbm, ku_hbm, vu_hbm, qe_hbm, ke_hbm, ve_hbm, w_hbm,
     out_ref,
-    mods, q_lat, kv, ctx, ctx_rope, gate_buf, tab_a, tab_b, gains, q_all, k_buf, v_buf, k_ctx, v_ctx, top_ref, acc_ref, att, held,
+    mods, gates, q_lat, kv, ctx, ctx_rope, gate_buf, tab_a, tab_b, gains, q_all, k_buf, v_buf, k_ctx, v_ctx, att, held,
     w_all, shift_w, scale_w, gate_w, tokens_ref, qd_ref, kd_ref, rd_ref,
     qu_raw, ku_raw, vu_raw, qe_ref, ke_ref, ve_ref, qu_ref, ku_ref, vu_ref,
-    load_sem, mod_send, mod_recv, q_send, q_recv, kv_send, kv_recv, c_send, c_recv, w_send, w_recv,
-    x_send, x_recv, a_send, a_recv,
+    load_sem, mod_send, mod_recv, g_send, g_recv, q_send, q_recv, kv_send, kv_recv, c_send, c_recv, w_send, w_recv,
+    z_send, z_recv, x_send, x_recv, a_send, a_recv, *state,
 ):
+    top_refs, acc_refs = state[:heads], state[heads:]
     s_me = lax.axis_index("sp")
     t_me = lax.axis_index("tp")
     d_me = lax.axis_index("dp")
     me = s_me * tp + t_me
-    half = mods.shape[2]
     rows = tokens_ref.shape[0]
     rank = ku_raw.shape[0]
     group = tp * rows
     ctx_rows = cl_hbm.shape[0]
-    share = w_hbm.shape[0] // dp
+    pair = 2 - sp % 2
+    share = w_hbm.shape[0] // (pair * dp)
     width = w_hbm.shape[1]
     pieces = rank // rows
 
@@ -163,15 +164,16 @@
         pl.semaphore_signal(barrier, inc=1, device_id=twin(e), device_id_type=MESH)
 
     with jax.named_scope("modmm"):
-        c = cond_ref[...].astype(F32)
+        c = cond_ref[...].reshape(1, cond_ref.shape[0]).astype(F32)
         act = (c / (1.0 + jnp.exp(-c))).astype(BF16)
         act = jnp.broadcast_to(act, (16, act.shape[1]))
         terms = []
         for i, w in enumerate((shift_w, scale_w, gate_w)):
             first[i].wait()
             term = jnp.dot(act, w[...], preferred_element_type=F32)[0:1]
-            terms += [term[:, :half], term[:, half:]]
-        mods[me] = jnp.concatenate(terms + [terms[0], terms[0]], axis=0)
+            terms.append([term[:, c : c + LANES] for c in range(0, term.shape[1], LANES)])
+        mods[me] = jnp.concatenate(terms[0] + terms[1], axis=0)
+        gates[me] = jnp.concatenate(terms[2], axis=0)
         for cp in ctx_load:
             cp.wait()
         w_load.wait()
@@ -182,25 +184,76 @@
     for i, (ds, dt) in enumerate(others):
         mod_copies.append(remote(mods.at[me], mods.at[me], mod_send.at[i], mod_recv.at[i], peer(ds, dt)))
         mod_copies[-1].start()
-    ctx_copies = []
-    for ds in range(1, sp):
-        for k, buf in enumerate((ctx, ctx_rope)):
-            i = 2 * ds - 2 + k
-            ctx_copies.append(remote(buf.at[0], buf.at[ds], c_send.at[i], c_recv.at[i], column(ds)))
-            ctx_copies[-1].start()
-
-    cut = share // 2
-    my_start = pl.multiple_of(d_me * share, share)
-
-    def w_copy(d, part):
-        span = pl.ds(pl.multiple_of(my_start + part * cut, cut), cut)
-        i = (d - 1) * 2 + part
-        return remote(w_all.at[0, span], w_all.at[d, span], w_send.at[i], w_recv.at[i], mate(d))
-
-    early = [(d, 0) for d in range(1, tp - 1)]
-    late = [(d, part) for d in range(1, tp) for part in range(2) if (d, part) not in early]
-    for d, part in early:
-        w_copy(d, part).start()
+
+    def gate_copy(i):
+        return remote(gates.at[me], gates.at[me], g_send.at[i], g_recv.at[i], peer(*others[i]))
+
+    def ctx_up(k):
+        device = {"sp": lax.rem(s_me + 1, sp)}
+        return [
+            remote(buf.at[k - 1], buf.at[k], c_send.at[j, k - 1], c_recv.at[j, k], device)
+            for j, buf in enumerate((ctx, ctx_rope))
+        ]
+
+    def ctx_down(k):
+        device = {"sp": lax.rem(s_me + sp - 1, sp)}
+        src = (sp - k + 1) % sp
+        return [
+            remote(buf.at[src], buf.at[sp - k], c_send.at[j, sp - 2 + k], c_recv.at[j, sp - k], device)
+            for j, buf in enumerate((ctx, ctx_rope))
+        ]
+
+    def ctx_phase(k, arrive=True, depart=True):
+        @pl.when(s_me >= k - 1)
+        def _():
+            if arrive and k > 1:
+                for cp in ctx_up(k - 1):
+                    cp.wait_recv()
+
+            @pl.when(s_me < sp - 1)
+            def _():
+                if depart and k < sp:
+                    for cp in ctx_up(k):
+                        cp.start()
+
+        @pl.when(s_me + k - 1 <= sp - 1)
+        def _():
+            if arrive and k > 1:
+                for cp in ctx_down(k - 1):
+                    cp.wait_recv()
+
+            @pl.when(s_me > 0)
+            def _():
+                if depart and k < sp:
+                    for cp in ctx_down(k):
+                        cp.start()
+
+    ctx_phase(1)
+
+    parity = lax.rem(s_me, pair)
+
+    def w_span(k):
+        return pl.ds(pl.multiple_of((k * dp + d_me) * share, share), share)
+
+    def w_copy(d):
+        return remote(
+            w_all.at[0, w_span(parity)], w_all.at[d, w_span(parity)], w_send.at[d - 1], w_recv.at[d - 1], mate(d)
+        )
+
+    def z_copy(d):
+        span = w_span(parity)
+        device = {"sp": s_me + 1 - 2 * parity}
+        return remote(w_all.at[d, span], w_all.at[d, span], z_send.at[d - 1], z_recv.at[d - 1], device)
+
+    def x_copy(d, e, k):
+        i = ((d - 1) * (dp - 1) + e - 1) * pair + k
+        span = w_span(k)
+        return remote(w_all.at[d, span], w_all.at[d, span], x_send.at[i], x_recv.at[i], twin(e))
+
+    early = range(1, tp - 1)
+    late = range(tp - 1, tp)
+    for d in early:
+        w_copy(d).start()
 
     with jax.named_scope("prep"):
         gains[...] = jnp.zeros(gains.shape, F32)
@@ -244,15 +297,23 @@
         for cp in mod_copies:
             cp.wait_recv()
     with jax.named_scope("stageB"):
-        parts = [[], [], []]
-        for t in range(tp):
-            total = mods[t]
-            for s in range(1, sp):
-                total = total + mods[s * tp + t]
-            for k in range(3):
-                parts[k] += [total[2 * k : 2 * k + 1], total[2 * k + 1 : 2 * k + 2]]
-        shift, scale, gate = [jnp.concatenate(p, axis=1) for p in parts]
-        gate_buf[...] = gate
+
+        def gathered(buf):
+            rows_of = []
+            for t in range(tp):
+                total = buf[t]
+                for s in range(1, sp):
+                    total = total + buf[s * tp + t]
+                rows_of.append(total)
+            return rows_of
+
+        def joined(totals, start):
+            count = width // tp // LANES
+            return jnp.concatenate([t[start + c : start + c + 1] for t in totals for c in range(count)], axis=1)
+
+        totals = gathered(mods)
+        shift = joined(totals, 0)
+        scale = joined(totals, width // tp // LANES)
         normed = (xn * (1.0 + scale) + shift).astype(BF16)
         q = jnp.dot(normed, qd_ref[...], preferred_element_type=F32)
         q_lat[0] = (q * norm_factor(q) * qg_ref[...]).astype(BF16)
@@ -283,88 +344,131 @@
 
     contract = (((1,), (1,)), ((), ()))
 
-    def expand(lat, rope_t, a, b, store):
-        rope = lax.dot_general(rope_t, spread, (((0,), (0,)), ((), ())), preferred_element_type=F32)
-        rope_square = jnp.sum(jnp.where(live, rope * rope, 0.0), axis=-1, keepdims=True)
-        turned = rope * a if b is None else rope * a + pltpu.roll(rope, QK_DIM, 1) * b
+    def expand(lats, ropes, a, b, store):
+        rope = [
+            lax.dot_general(r, spread, (((0,), (0,)), ((), ())), preferred_element_type=F32) for r in ropes
+        ]
+        rope = jnp.concatenate(rope, axis=0)
+        lat = jnp.concatenate(lats, axis=0)
         k = jnp.dot(lat, ku_ref[...], preferred_element_type=F32)
         v = jnp.dot(lat, vu_ref[...], preferred_element_type=F32)
+        k = [k[:, h * LANES : (h + 1) * LANES] for h in range(heads)]
+        rope_square = jnp.sum(jnp.where(live, rope * rope, 0.0), axis=-1, keepdims=True)
+        squares = [jnp.sum(kh * kh, axis=-1, keepdims=True) + rope_square for kh in k]
+        turned = rope * a if b is None else rope * a + pltpu.roll(rope, QK_DIM, 1) * b
+        scales = [lax.rsqrt(square * (1.0 / QK_DIM) + EPS) for square in squares]
         for h in range(heads):
-            cols = slice(h * LANES, (h + 1) * LANES)
-            kh = k[:, cols]
-            square = jnp.sum(kh * kh, axis=-1, keepdims=True) + rope_square
-            scale_h = lax.rsqrt(square * (1.0 / QK_DIM) + EPS)
-            store(h, ((kh * kgain + turned) * scale_h).astype(BF16), (v[:, cols] + ones_lane).astype(BF16))
-
-    def attend(start, count, keys, values, h, lift, fresh):
-        span = pl.ds(start, count)
-        s = lax.dot_general(q_all[h, span, :], keys, contract, preferred_element_type=F32)
-        peak = jnp.max(s, axis=-1, keepdims=True)
-        if lift is not None:
-            peak = peak + lift
-        if fresh:
-            top = jnp.broadcast_to(peak, (count, LANES))
-        else:
-            old = top_ref[h, span, :]
-            top = jnp.maximum(old, peak)
-        top_ref[h, span, :] = top
-        floor = top if lift is None else top - lift
-        p = jnp.exp2(s - jnp.concatenate([floor] * (keys.shape[0] // LANES), axis=1)).astype(BF16)
-        add = jnp.dot(p, values, preferred_element_type=F32)
-        if not fresh:
-            add = acc_ref[h, span, :] * jnp.exp2(old - top) + add
-        acc_ref[h, span, :] = add
+            store(
+                h, ((k[h] * kgain + turned) * scales[h]).astype(BF16),
+                (v[:, h * LANES : (h + 1) * LANES] + ones_lane).astype(BF16),
+            )
+
+    def attend(starts, k_ref, v_ref, first_key, keys, lift, fresh):
+        key_span = pl.ds(first_key, keys)
+        items = [(pl.ds(start, q_rows), h) for start in starts for h in range(heads)]
+
+        def product(span, h):
+            return lax.dot_general(q_all[h, span, :], k_ref[h, key_span, :], contract, preferred_element_type=F32)
+
+        ahead = 2
+        scores = [product(*item) for item in items[:ahead]]
+        for i, (span, h) in enumerate(items):
+            if i + ahead < len(items):
+                scores.append(product(*items[i + ahead]))
+            s = scores[i]
+            peak = jnp.max(s, axis=-1, keepdims=True)
+            if lift:
+                lift_h = lift_ref[h] * LOG2E
+                peak = peak + lift_h
+            if fresh:
+                top = jnp.broadcast_to(peak, (q_rows, LANES))
+            else:
+                old = top_refs[h][span, :]
+                top = jnp.maximum(old, peak)
+            floor = top - lift_h if lift else top
+            p = jnp.exp2(s - jnp.concatenate([floor] * (keys // LANES), axis=1)).astype(BF16)
+            add = jnp.dot(p, v_ref[h, key_span, :], preferred_element_type=F32)
+            if not fresh:
+                add = acc_refs[h][span, :] * jnp.exp2(old - top) + add
+            top_refs[h][span, :] = top
+            acc_refs[h][span, :] = add
+
+    def expand_context(first, count):
+        slots = []
+        for i in range(first, first + count):
+            if i == 0:
+                slots.append(0)
+            elif i == 1:
+                slots.append(jnp.where(s_me == 0, sp - 1, 1))
+            else:
+                slots.append(jnp.where(s_me == 0, i - 1, i))
+
+        def store(h, k, v):
+            k_ctx[h, first * ctx_rows : (first + count) * ctx_rows, :] = k
+            v_ctx[h, first * ctx_rows : (first + count) * ctx_rows, :] = v
+
+        expand([ctx[slot] for slot in slots], [ctx_rope[slot] for slot in slots], kgain, None, store)
+
+    def tables(source, d, gain, gain_swap):
+        start = pl.multiple_of((source * tp + (partner(tp, t_me, d) if d else t_me)) * rows, rows)
+        return tab_a[pl.ds(start, rows), :] * gain, tab_b[pl.ds(start, rows), :] * gain_swap
+
+    def stacked(pieces_of):
+        return [jnp.concatenate(p, axis=0) for p in zip(*pieces_of)]
+
+    def queries(mates):
+        a, b = stacked([tables(s_me, d, qgain, qgain_swap) for d in mates])
+        qx = jnp.dot(jnp.concatenate([q_lat[d] for d in mates], axis=0), qu_ref[...], preferred_element_type=F32)
+        qx = [qx[:, h * LANES : (h + 1) * LANES] for h in range(heads)]
+        squares = [jnp.sum(jnp.where(live, v * v, 0.0), axis=-1, keepdims=True) for v in qx]
+        turned = [v * a + pltpu.roll(v, QK_DIM, 1) * b for v in qx]
+        scales = [lax.rsqrt(square * (1.0 / QK_DIM) + EPS) * factor for square in squares]
+        slot = (tp - 1 - mates[0]) * rows
+        for h in range(heads):
+            q_all[h, slot : slot + len(mates) * rows, :] = (turned[h] * scales[h]).astype(BF16)
+
+    near = min(2, sp)
+    near_keys = near * ctx_rows
+    far_keys = (sp - near) * ctx_rows
+    q_rows = 2 * rows if tp % 2 == 0 else rows
 
     with jax.named_scope("ctxwait"):
-        for cp in ctx_copies:
-            cp.wait_recv()
+        ctx_phase(2)
     with jax.named_scope("ctxexpand"):
-        def context_block(i, carry):
-            lat = ctx[i]
-            rope_t = ctx_rope[i]
-
-            def store(h, k, v):
-                span = pl.ds(pl.multiple_of(i * ctx_rows, ctx_rows), ctx_rows)
-                k_ctx[h, span, :] = k
-                v_ctx[h, span, :] = v
-
-            expand(lat, rope_t, kgain, None, store)
-            return carry
-
-        lax.fori_loop(0, sp, context_block, 0)
-
-    for d in range(tp):
-        slot = (tp - 1 - d) * rows
+        expand_context(0, near)
+    for first_mate in range(0, tp, q_rows // rows):
+        mates = list(range(first_mate + q_rows // rows - 1, first_mate - 1, -1))
         with jax.named_scope("qwait"):
-            if d:
-                q_copy(d).wait_recv()
-        with jax.named_scope("qctx"):
-            start = pl.multiple_of((s_me * tp + (partner(tp, t_me, d) if d else t_me)) * rows, rows)
-            a = tab_a[pl.ds(start, rows), :] * qgain
-            b = tab_b[pl.ds(start, rows), :] * qgain_swap
-            qx = jnp.dot(q_lat[d], qu_ref[...], preferred_element_type=F32)
-            for h in range(heads):
-                v = qx[:, h * LANES : (h + 1) * LANES]
-                square = jnp.sum(jnp.where(live, v * v, 0.0), axis=-1, keepdims=True)
-                scale_h = lax.rsqrt(square * (1.0 / QK_DIM) + EPS) * factor
-                q_all[h, slot : slot + rows, :] = ((v * a + pltpu.roll(v, QK_DIM, 1) * b) * scale_h).astype(BF16)
-            for h in range(heads):
-                attend(slot, rows, k_ctx[h], v_ctx[h], h, lift_ref[h] * LOG2E, True)
-
-    with jax.named_scope("zwait"):
-        for ds in range(1, sp):
-            kv_column(ds).wait_recv()
-            for d in range(1, tp):
-                kv_mate(ds, d).start()
-    for d, part in late:
-        w_copy(d, part).start()
-
-    def x_copy(d, e):
-        i = (d - 1) * (dp - 1) + e - 1
-        span = pl.ds(my_start, share)
-        return remote(w_all.at[d, span], w_all.at[d, span], x_send.at[i], x_recv.at[i], twin(e))
-
-    q_rows = 2 * rows if tp % 2 == 0 else rows
+            for d in reversed(mates):
+                if d:
+                    q_copy(d).wait_recv()
+        with jax.named_scope("queries"):
+            queries(mates)
+        with jax.named_scope("ctxattend"):
+            attend([(tp - 1 - mates[0]) * rows], k_ctx, v_ctx, 0, near_keys, True, True)
+        if first_mate == 0:
+            with jax.named_scope("ctxwait3"):
+                ctx_phase(3)
+            with jax.named_scope("zwait"):
+                for ds in range(1, sp):
+                    kv_column(ds).wait_recv()
+                    for m in range(1, tp):
+                        kv_mate(ds, m).start()
+    for i in range(len(others)):
+        gate_copy(i).start()
+    for d in late:
+        w_copy(d).start()
+    with jax.named_scope("ctxwait4"):
+        for k in range(4, sp + 1):
+            ctx_phase(k)
+    if pair > 1:
+        with jax.named_scope("wearly"):
+            for d in early:
+                w_copy(d).wait_recv()
+                z_copy(d).start()
+    if far_keys:
+        with jax.named_scope("ctxexpand"):
+            expand_context(near, sp - near)
 
     def group_step(i, carry):
         ds = lax.rem(lax.rem(i, 2) * ((i + 1) // 2) + lax.rem(i + 1, 2) * (sp - i // 2), sp)
@@ -373,42 +477,50 @@
             for d in range(1, tp):
                 kv_mate(ds, d).wait_recv()
         with jax.named_scope("kvexpand"):
-            for d in range(tp):
-                start = pl.multiple_of((source * tp + (partner(tp, t_me, d) if d else t_me)) * rows, rows)
-                a = tab_a[pl.ds(start, rows), :] * kgain
-                b = tab_b[pl.ds(start, rows), :] * kgain_swap
-                lat = kv[ds, d, pl.ds(0, rows), :]
-                tail = kv[ds, d, pl.ds(rows, ROPE_DIM // pieces), :]
-                rope_t = jnp.concatenate([tail[:, p * rows : (p + 1) * rows] for p in range(pieces)], axis=0)
-
-                def store(h, k, v):
-                    k_buf[h, d * rows : (d + 1) * rows, :] = k
-                    v_buf[h, d * rows : (d + 1) * rows, :] = v
-
-                expand(lat, rope_t, a, b, store)
+            a, b = stacked([tables(source, d, kgain, kgain_swap) for d in range(tp)])
+            tails = [kv[ds, d, pl.ds(rows, ROPE_DIM // pieces), :] for d in range(tp)]
+            ropes = [
+                jnp.concatenate([t[:, p * rows : (p + 1) * rows] for p in range(pieces)], axis=0) for t in tails
+            ]
+
+            def store(h, k, v):
+                k_buf[h] = k
+                v_buf[h] = v
+
+            expand([kv[ds, d, pl.ds(0, rows), :] for d in range(tp)], ropes, a, b, store)
 
         with jax.named_scope("attend"):
-
-            def rows_step(j, inner):
-                start = pl.multiple_of(j * q_rows, q_rows)
-                for h in range(heads):
-                    attend(start, q_rows, k_buf[h], v_buf[h], h, None, False)
-                return inner
-
-            lax.fori_loop(0, group // q_rows, rows_step, 0)
+            attend(range(0, group, q_rows), k_buf, v_buf, 0, group, False, False)
+
+        if far_keys:
+
+            @pl.when(i == 0)
+            def _():
+                with jax.named_scope("ctxattend"):
+                    attend(range(0, group, q_rows), k_ctx, v_ctx, near_keys, far_keys, True, False)
 
         @pl.when(i == sp - 2)
         def _():
             with jax.named_scope("wswap"):
-                for d in range(1, tp):
-                    for part in range(2):
-                        w_copy(d, part).wait_recv()
-                    for e in range(1, dp):
-                        x_copy(d, e).start()
+                for d in late:
+                    w_copy(d).wait_recv()
+                    if pair > 1:
+                        z_copy(d).start()
+                if pair == 1:
+                    for d in early:
+                        w_copy(d).wait_recv()
 
         return carry
 
     lax.fori_loop(0, sp, group_step, 0)
+
+    with jax.named_scope("wtwin"):
+        for d in range(1, tp):
+            if pair > 1:
+                z_copy(d).wait_recv()
+            for e in range(1, dp):
+                for k in range(pair):
+                    x_copy(d, e, k).start()
 
     def a_copy(d):
         return remote(att.at[d], held.at[d - 1], a_send.at[d - 1], a_recv.at[d - 1], mate(d))
@@ -418,7 +530,7 @@
             slot = (tp - 1 - d) * rows
             outs = []
             for h in range(heads):
-                total = acc_ref[h, slot : slot + rows, :]
+                total = acc_refs[h][slot : slot + rows, :]
                 outs.append((total[:, :VALUE_DIM] / total[:, VALUE_DIM : VALUE_DIM + 1]).astype(BF16))
             att[d] = jnp.concatenate(outs, axis=1)
             if d:
@@ -433,25 +545,45 @@
         for d in range(1, tp):
             with jax.named_scope("xwait"):
                 for e in range(1, dp):
-                    x_copy(d, e).wait_recv()
+                    for k in range(pair):
+                        x_copy(d, e, k).wait_recv()
             with jax.named_scope("await"):
                 a_copy(d).wait_recv()
             for n, cols in enumerate(spans):
                 term = jnp.dot(held[d - 1], w_all[d, :, cols], preferred_element_type=F32)
                 mixed[n] = mixed[n] + term.astype(BF16).astype(F32)
+        for i in range(len(others)):
+            gate_copy(i).wait_recv()
+        gate_buf[...] = joined(gathered(gates), 0)
         for n, cols in enumerate(spans):
             out_ref[:, cols] = (tokens_ref[:, cols].astype(F32) + gate_buf[:, cols] * mixed[n]).astype(BF16)
 
     with jax.named_scope("drain"):
-        for cp in mod_copies + ctx_copies:
+        for cp in mod_copies:
             cp.wait_send()
+        for i in range(len(others)):
+            gate_copy(i).wait_send()
+        for k in range(1, sp):
+
+            @pl.when((s_me >= k - 1) & (s_me < sp - 1))
+            def _():
+                for cp in ctx_up(k):
+                    cp.wait_send()
+
+            @pl.when((s_me + k - 1 <= sp - 1) & (s_me > 0))
+            def _():
+                for cp in ctx_down(k):
+                    cp.wait_send()
+
         for d in range(1, tp):
             q_copy(d).wait_send()
             a_copy(d).wait_send()
-            for part in range(2):
-                w_copy(d, part).wait_send()
+            w_copy(d).wait_send()
+            if pair > 1:
+                z_copy(d).wait_send()
             for e in range(1, dp):
-                x_copy(d, e).wait_send()
+                for k in range(pair):
+                    x_copy(d, e, k).wait_send()
             for ds in range(sp):
                 kv_mate(ds, d).wait_send()
         for ds in range(1, sp):
@@ -482,11 +614,12 @@
     vmem = pltpu.VMEM
     return pl.pallas_call(
         functools.partial(fused_kernel, sp, tp, dp, heads),
-        out_shape=jax.ShapeDtypeStruct((rows, width), BF16),
-        in_specs=[VMEM_SPEC] * 6 + [pl.BlockSpec(memory_space=pltpu.SMEM)] + [VMEM_SPEC] * 5 + [ANY_SPEC] * 16,
+        out_shape=pltpu.VMEM((rows, width), BF16),
+        in_specs=[VMEM_SPEC] * 6 + [pl.BlockSpec(memory_space=pltpu.SMEM)] + [VMEM_SPEC] * 5 + [HBM_SPEC] * 16,
         out_specs=VMEM_SPEC,
         scratch_shapes=[
-            vmem((n_dev, 8, width // tp // 2), F32),
+            vmem((n_dev, 2 * width // tp // LANES, LANES), F32),
+            vmem((n_dev, width // tp // LANES, LANES), F32),
             vmem((tp, rows, q_rank), BF16),
             vmem((sp, tp, rows + ROPE_DIM * rows // rank, rank), BF16),
             vmem((sp, ctx_rows, rank), BF16),
@@ -500,8 +633,6 @@
             vmem((heads, group, LANES), BF16),
             vmem((heads, context, LANES), BF16),
             vmem((heads, context, LANES), BF16),
-            vmem((heads, group, LANES), F32),
-            vmem((heads, group, LANES), F32),
             vmem((tp, rows, heads * VALUE_DIM), BF16),
             vmem((tp - 1, rows, heads * VALUE_DIM), BF16),
             vmem((tp,) + out_weight.shape, BF16),
@@ -523,19 +654,22 @@
             vmem((rank, heads * LANES), BF16),
             dma((16,)),
             dma((n_dev - 1,)), dma((n_dev - 1,)),
+            dma((n_dev - 1,)), dma((n_dev - 1,)),
             dma((tp - 1,)), dma((tp - 1,)),
             dma((sp, tp)), dma((sp, tp)),
-            dma((2 * (sp - 1),)), dma((2 * (sp - 1),)),
-            dma((2 * (tp - 1),)), dma((2 * (tp - 1),)),
-            dma(((tp - 1) * (dp - 1),)), dma(((tp - 1) * (dp - 1),)),
+            dma((2, 2 * sp)), dma((2, sp)),
             dma((tp - 1,)), dma((tp - 1,)),
-        ],
+            dma((tp - 1,)), dma((tp - 1,)),
+            dma((2 * (tp - 1) * (dp - 1),)), dma((2 * (tp - 1) * (dp - 1),)),
+            dma((tp - 1,)), dma((tp - 1,)),
+        ]
+        + [vmem((group, LANES), F32)] * (2 * heads),
         compiler_params=pltpu.CompilerParams(
-            collective_id=0, has_side_effects=True, vmem_limit_bytes=60 * 1024 * 1024
+            collective_id=0, has_side_effects=True, vmem_limit_bytes=58 * 1024 * 1024
         ),
         name="fused",
     )(
-        condition[None], norm_gain[None], query_gain[None], kv_gain[None], query_norm_gain[None], key_norm_gain[None],
+        condition, norm_gain[None], query_gain[None], kv_gain[None], query_norm_gain[None], key_norm_gain[None],
         context_lift, jnp.asarray(row_a), jnp.asarray(row_b), jnp.asarray(col_a), jnp.asarray(col_b),
         jnp.asarray(rope_spread(), BF16),
         shift_weight, scale_weight, gate_weight, latent_tokens, query_down, kv_down, rope_down.T,

time: 77.1 us -> 53.7 us (0.70)
  Pallas kernels: 73.3 us -> 52.7 us
  local copies, waits for them, and re-layouts: 3.14 us -> 0.8 us
    pallas_call x1, Pallas kernels: 73.3 us -> 52.7 us  [local(): pl.pallas_call(functools.partial(fused_kernel, sp, tp, dp, heads), out_sh...]
    broadcast_in_dim x1 -> x0, local copies, waits for them, and re-layouts: 1.26 us -> none  [local(): condition[None]]
    unnamed x1, local copies, waits for them, and re-layouts: 1.88 us -> 0.8 us
where the time goes in v2:
time: 53.7 us; the launch traced here: 53.5 us
  Pallas kernels  52.7 us (98%)
  local copies, waits for them, and re-layouts  0.8 us (1%)
    pallas_call x1, Pallas kernels, local(): pl.pallas_call(functools.partial(fused_kernel, sp, tp, dp, heads), out_sh...  52.7 us

profile of v2, /device:TPU:0, one launch (start us, length us, event | category | flops | bytes accessed | tf_op | source)
XLA Modules:
  0.0 53.5 jit_solution(1513611191816431296)
XLA Ops:
  0.0 52.7 %fused.1 = bf16[128,2048]{1,0:T(8,128)(2,1)S(1)} custom-call(bf16[512]{0:T(512)(128)(2,1)} %cond_ref.1, f32[1,2048]{1,0:T(1,128)} %bitcast.9, f32[1,512]{1,0:T(1,128)} %bitcast.10, f32[1,256]{1,0:T(1,128)} %bitcast.11, f32[1,96]{1,0:T(1,128)} %bitcast.12, f32[1,96]{1,0:T(1,128)} %bitcast.13, f32[4]{0:T(128)} %lift_ref.1, f32[32,128]{1,0:T(8,128)} %constant.16.clone.row_a, ...), custom_call_target="tpu_custom_call" | custom-call | tf_op jit(solution)/shard_map/fused/pallas_call | solution.py:615
  52.7 0.8 %copy.30 = bf16[128,2048]{1,0:T(8,128)(2,1)} copy(bf16[128,2048]{1,0:T(8,128)(2,1)S(1)} %fused.1) | data formatting | bytes 1048576

commit v3 on v2

--- a/solution.py
+++ b/solution.py
@@ -92,15 +92,17 @@
 
 def fused_kernel(
     sp, tp, dp, heads,
-    cond_ref, gain_ref, qg_ref, kg_ref, qgain_ref, kgain_ref, lift_ref, row_a, row_b, col_a, col_b, spread_ref,
+    lift_ref, cond_hbm, gain_hbm, qg_hbm, kg_hbm, qgain_hbm, kgain_hbm, row_a_hbm, row_b_hbm, col_a_hbm, col_b_hbm,
+    spread_hbm,
     shift_hbm, scale_hbm, gate_hbm, tokens_hbm, qd_hbm, kd_hbm, rd_hbm, cl_hbm, cr_hbm,
     qu_hbm, ku_hbm, vu_hbm, qe_hbm, ke_hbm, ve_hbm, w_hbm,
     out_ref,
     mods, gates, q_lat, kv, ctx, ctx_rope, gate_buf, tab_a, tab_b, gains, q_all, k_buf, v_buf, k_ctx, v_ctx, att, held,
     w_all, shift_w, scale_w, gate_w, tokens_ref, qd_ref, kd_ref, rd_ref,
     qu_raw, ku_raw, vu_raw, qe_ref, ke_ref, ve_ref, qu_ref, ku_ref, vu_ref,
+    cond_ref, gain_ref, qg_ref, kg_ref, qgain_ref, kgain_ref, row_a, row_b, col_a, col_b, spread_ref,
     load_sem, mod_send, mod_recv, g_send, g_recv, q_send, q_recv, kv_send, kv_recv, c_send, c_recv, w_send, w_recv,
-    z_send, z_recv, x_send, x_recv, a_send, a_recv, *state,
+    r_send, r_recv, z_send, z_recv, x_send, x_recv, a_send, a_recv, *state,
 ):
     top_refs, acc_refs = state[:heads], state[heads:]
     s_me = lax.axis_index("sp")
@@ -112,7 +114,10 @@
     group = tp * rows
     ctx_rows = cl_hbm.shape[0]
     pair = 2 - sp % 2
-    share = w_hbm.shape[0] // (pair * dp)
+    share = w_hbm.shape[0] // dp
+    unit = share // 4
+    relay = tp == 4
+    direct = range(1, 3) if relay else range(1, tp)
     width = w_hbm.shape[1]
     pieces = rank // rows
 
@@ -121,6 +126,7 @@
         cp.start()
         return cp
 
+    cond_load = load(16, cond_hbm, cond_ref)
     first = [
         load(i, src, dst)
         for i, (src, dst) in enumerate(((shift_hbm, shift_w), (scale_hbm, scale_w), (gate_hbm, gate_w)))
@@ -129,15 +135,26 @@
         load(3, cl_hbm, ctx.at[0]),
         load(4, cr_hbm, ctx_rope.at[0]),
     ]
-    w_load = load(5, w_hbm, w_all.at[0])
-    token_load = load(6, tokens_hbm, tokens_ref)
-    down_load = [load(7, qd_hbm, qd_ref), load(8, kd_hbm, kd_ref), load(9, rd_hbm, rd_ref)]
-    up_load = [
-        load(10 + i, src, dst)
-        for i, (src, dst) in enumerate((
-            (qu_hbm, qu_raw), (ku_hbm, ku_raw), (vu_hbm, vu_raw), (qe_hbm, qe_ref), (ke_hbm, ke_ref), (ve_hbm, ve_ref),
-        ))
-    ]
+
+    def later_loads():
+        w_load = load(5, w_hbm, w_all.at[0])
+        small_load = [
+            load(17 + i, src, dst)
+            for i, (src, dst) in enumerate((
+                (gain_hbm, gain_ref), (qg_hbm, qg_ref), (kg_hbm, kg_ref), (qgain_hbm, qgain_ref),
+                (kgain_hbm, kgain_ref), (row_a_hbm, row_a), (row_b_hbm, row_b), (col_a_hbm, col_a),
+                (col_b_hbm, col_b), (spread_hbm, spread_ref),
+            ))
+        ]
+        token_load = load(6, tokens_hbm, tokens_ref)
+        up_load = [
+            load(10 + i, src, dst)
+            for i, (src, dst) in enumerate((
+                (qu_hbm, qu_raw), (ku_hbm, ku_raw), (vu_hbm, vu_raw), (qe_hbm, qe_ref), (ke_hbm, ke_ref), (ve_hbm, ve_ref),
+            ))
+        ]
+        down_load = [load(7, qd_hbm, qd_ref), load(8, kd_hbm, kd_ref), load(9, rd_hbm, rd_ref)]
+        return w_load, small_load, token_load, up_load, down_load
 
     def peer(ds, dt):
         return {"sp": lax.rem(s_me + ds, sp), "tp": lax.rem(t_me + dt, tp)}
@@ -164,19 +181,21 @@
         pl.semaphore_signal(barrier, inc=1, device_id=twin(e), device_id_type=MESH)
 
     with jax.named_scope("modmm"):
+        cond_load.wait()
         c = cond_ref[...].reshape(1, cond_ref.shape[0]).astype(F32)
         act = (c / (1.0 + jnp.exp(-c))).astype(BF16)
         act = jnp.broadcast_to(act, (16, act.shape[1]))
         terms = []
         for i, w in enumerate((shift_w, scale_w, gate_w)):
             first[i].wait()
+            if i == 2:
+                w_load, small_load, token_load, up_load, down_load = later_loads()
             term = jnp.dot(act, w[...], preferred_element_type=F32)[0:1]
             terms.append([term[:, c : c + LANES] for c in range(0, term.shape[1], LANES)])
         mods[me] = jnp.concatenate(terms[0] + terms[1], axis=0)
         gates[me] = jnp.concatenate(terms[2], axis=0)
         for cp in ctx_load:
             cp.wait()
-        w_load.wait()
 
     with jax.named_scope("barrier"):
         pl.semaphore_wait(barrier, len(others) + dp - 1)
@@ -231,31 +250,49 @@
     ctx_phase(1)
 
     parity = lax.rem(s_me, pair)
-
-    def w_span(k):
-        return pl.ds(pl.multiple_of((k * dp + d_me) * share, share), share)
-
-    def w_copy(d):
+    base = d_me * share
+    mine = [parity * 3 * unit, unit, 2 * unit] if pair > 1 else [k * unit for k in range(4)]
+
+    def w_rows(offset):
+        return pl.ds(pl.multiple_of(base + offset, unit), unit)
+
+    def w_copy(d, j):
+        span = w_rows(mine[j])
+        return remote(w_all.at[0, span], w_all.at[d, span], w_send.at[d - 1, j], w_recv.at[d - 1, j], mate(d))
+
+    def w_relay(j, k):
+        span = w_rows(mine[j])
+        cols = pl.ds(k * (width // 2), width // 2)
         return remote(
-            w_all.at[0, w_span(parity)], w_all.at[d, w_span(parity)], w_send.at[d - 1], w_recv.at[d - 1], mate(d)
+            w_all.at[1 + k, span, cols], w_all.at[3, span, cols], r_send.at[j, k], r_recv.at[j, k], mate(2 - k)
         )
 
     def z_copy(d):
-        span = w_span(parity)
+        span = w_rows(mine[0])
         device = {"sp": s_me + 1 - 2 * parity}
         return remote(w_all.at[d, span], w_all.at[d, span], z_send.at[d - 1], z_recv.at[d - 1], device)
 
-    def x_copy(d, e, k):
-        i = ((d - 1) * (dp - 1) + e - 1) * pair + k
-        span = w_span(k)
-        return remote(w_all.at[d, span], w_all.at[d, span], x_send.at[i], x_recv.at[i], twin(e))
-
-    early = range(1, tp - 1)
-    late = range(tp - 1, tp)
-    for d in early:
-        w_copy(d).start()
+    def x_copy(d, e, j):
+        span = w_rows(mine[j] if j < len(mine) else (1 - parity) * 3 * unit)
+        i = (d - 1) * (dp - 1) + e - 1
+        return remote(w_all.at[d, span], w_all.at[d, span], x_send.at[i, j], x_recv.at[i, j], twin(e))
+
+    def w_arrive(d, j):
+        if relay and d == 3:
+            for k in range(2):
+                w_relay(j, k).wait_recv()
+        else:
+            w_copy(d, j).wait_recv()
+
+    early = range(2)
+    late = range(2, len(mine))
+    w_load.wait()
+    for d in direct:
+        w_copy(d, 0).start()
 
     with jax.named_scope("prep"):
+        for cp in small_load:
+            cp.wait()
         gains[...] = jnp.zeros(gains.shape, F32)
         gains[0:1, :QK_DIM] = qgain_ref[...]
         gains[1:2, :QK_DIM] = kgain_ref[...]
@@ -296,6 +333,15 @@
     with jax.named_scope("waitmods"):
         for cp in mod_copies:
             cp.wait_recv()
+    def q_copy(d):
+        return remote(q_lat.at[0], q_lat.at[d], q_send.at[d - 1], q_recv.at[d - 1], mate(d))
+
+    def q_relay(k):
+        cols = pl.ds(k * (q_lat.shape[2] // 2), q_lat.shape[2] // 2)
+        return remote(
+            q_lat.at[1 + k, :, cols], q_lat.at[3, :, cols], q_send.at[2 + k], q_recv.at[2 + k], mate(2 - k)
+        )
+
     with jax.named_scope("stageB"):
 
         def gathered(buf):
@@ -317,6 +363,8 @@
         normed = (xn * (1.0 + scale) + shift).astype(BF16)
         q = jnp.dot(normed, qd_ref[...], preferred_element_type=F32)
         q_lat[0] = (q * norm_factor(q) * qg_ref[...]).astype(BF16)
+        for d in direct:
+            q_copy(d).start()
         lat = jnp.dot(normed, kd_ref[...], preferred_element_type=F32)
         kv[0, 0, :rows, :] = (lat * norm_factor(lat) * kg_ref[...]).astype(BF16)
         rope = lax.dot_general(
@@ -326,20 +374,30 @@
         for p in range(pieces):
             kv[0, 0, rows:, p * rows : (p + 1) * rows] = rope[p * piece : (p + 1) * piece]
 
-    def q_copy(d):
-        return remote(q_lat.at[0], q_lat.at[d], q_send.at[d - 1], q_recv.at[d - 1], mate(d))
-
     def kv_column(ds):
         return remote(kv.at[0, 0], kv.at[ds, 0], kv_send.at[ds, 0], kv_recv.at[ds, 0], column(ds))
 
     def kv_mate(ds, d):
         return remote(kv.at[ds, 0], kv.at[ds, d], kv_send.at[ds, d], kv_recv.at[ds, d], mate(d))
 
-    for d in range(1, tp):
-        q_copy(d).start()
-    for ds in range(1, sp):
-        kv_column(ds).start()
-    for d in range(1, tp):
+    def kv_relay(ds, k):
+        cols = pl.ds(k * (rank // 2), rank // 2)
+        return remote(
+            kv.at[ds, 1 + k, :, cols], kv.at[ds, 3, :, cols], kv_send.at[ds, 3 + k], kv_recv.at[ds, 3 + k], mate(2 - k)
+        )
+
+    def middle(i):
+        return (i + 1) // 2 if i % 2 else sp - i // 2
+
+    def source_step(i):
+        return jnp.where(s_me == 0, sp - i, jnp.where(s_me == sp - 1, i, middle(i)))
+
+    def target_step(i):
+        return jnp.where(s_me == 0, i, jnp.where(s_me == sp - 1, sp - i, middle(i)))
+
+    for i in range(1, sp):
+        kv_column(target_step(i)).start()
+    for d in direct:
         kv_mate(0, d).start()
 
     contract = (((1,), (1,)), ((), ()))
@@ -436,97 +494,71 @@
         ctx_phase(2)
     with jax.named_scope("ctxexpand"):
         expand_context(0, near)
-    for first_mate in range(0, tp, q_rows // rows):
+    def kv_relays(ds):
+        if relay:
+            for k in range(2):
+                kv_mate(ds, 1 + k).wait_recv()
+                kv_relay(ds, k).start()
+
+    def queries_attend(first_mate):
         mates = list(range(first_mate + q_rows // rows - 1, first_mate - 1, -1))
-        with jax.named_scope("qwait"):
-            for d in reversed(mates):
-                if d:
-                    q_copy(d).wait_recv()
         with jax.named_scope("queries"):
             queries(mates)
         with jax.named_scope("ctxattend"):
             attend([(tp - 1 - mates[0]) * rows], k_ctx, v_ctx, 0, near_keys, True, True)
-        if first_mate == 0:
-            with jax.named_scope("ctxwait3"):
-                ctx_phase(3)
-            with jax.named_scope("zwait"):
-                for ds in range(1, sp):
-                    kv_column(ds).wait_recv()
-                    for m in range(1, tp):
-                        kv_mate(ds, m).start()
+
+    with jax.named_scope("qwait"):
+        for d in direct:
+            q_copy(d).wait_recv()
+            if relay:
+                q_relay(d - 1).start()
+        if relay:
+            for k in range(2):
+                w_copy(1 + k, 0).wait_recv()
+                w_relay(0, k).start()
+    for d in direct:
+        w_copy(d, 1).start()
+    queries_attend(0)
+    with jax.named_scope("kvwait0"):
+        kv_relays(0)
+    with jax.named_scope("zwait"):
+        for i in range(1, sp):
+            ds = source_step(i)
+            kv_column(ds).wait_recv()
+            for d in direct:
+                kv_mate(ds, d).start()
     for i in range(len(others)):
         gate_copy(i).start()
-    for d in late:
-        w_copy(d).start()
-    with jax.named_scope("ctxwait4"):
-        for k in range(4, sp + 1):
-            ctx_phase(k)
+    with jax.named_scope("qwait3"):
+        if relay:
+            for k in range(2):
+                q_relay(k).wait_recv()
+    for first_mate in range(q_rows // rows, tp, q_rows // rows):
+        queries_attend(first_mate)
+    with jax.named_scope("ctxwait3"):
+        ctx_phase(3)
     if pair > 1:
-        with jax.named_scope("wearly"):
-            for d in early:
-                w_copy(d).wait_recv()
+        with jax.named_scope("pairwait"):
+            for d in direct:
+                if not relay:
+                    w_copy(d, 0).wait_recv()
                 z_copy(d).start()
-    if far_keys:
-        with jax.named_scope("ctxexpand"):
-            expand_context(near, sp - near)
-
-    def group_step(i, carry):
-        ds = lax.rem(lax.rem(i, 2) * ((i + 1) // 2) + lax.rem(i + 1, 2) * (sp - i // 2), sp)
-        source = lax.rem(s_me + sp - ds, sp)
-        with jax.named_scope("kvwait"):
-            for d in range(1, tp):
-                kv_mate(ds, d).wait_recv()
-        with jax.named_scope("kvexpand"):
-            a, b = stacked([tables(source, d, kgain, kgain_swap) for d in range(tp)])
-            tails = [kv[ds, d, pl.ds(rows, ROPE_DIM // pieces), :] for d in range(tp)]
-            ropes = [
-                jnp.concatenate([t[:, p * rows : (p + 1) * rows] for p in range(pieces)], axis=0) for t in tails
-            ]
-
-            def store(h, k, v):
-                k_buf[h] = k
-                v_buf[h] = v
-
-            expand([kv[ds, d, pl.ds(0, rows), :] for d in range(tp)], ropes, a, b, store)
-
-        with jax.named_scope("attend"):
-            attend(range(0, group, q_rows), k_buf, v_buf, 0, group, False, False)
-
-        if far_keys:
-
-            @pl.when(i == 0)
-            def _():
-                with jax.named_scope("ctxattend"):
-                    attend(range(0, group, q_rows), k_ctx, v_ctx, near_keys, far_keys, True, False)
-
-        @pl.when(i == sp - 2)
-        def _():
-            with jax.named_scope("wswap"):
-                for d in late:
-                    w_copy(d).wait_recv()
-                    if pair > 1:
-                        z_copy(d).start()
-                if pair == 1:
-                    for d in early:
-                        w_copy(d).wait_recv()
-
-        return carry
-
-    lax.fori_loop(0, sp, group_step, 0)
-
-    with jax.named_scope("wtwin"):
-        for d in range(1, tp):
-            if pair > 1:
-                z_copy(d).wait_recv()
-            for e in range(1, dp):
-                for k in range(pair):
-                    x_copy(d, e, k).start()
+    with jax.named_scope("relaywait"):
+        for i in range(1, min(3, sp)):
+            kv_relays(source_step(i))
+        if relay:
+            for k in range(2):
+                w_copy(1 + k, 1).wait_recv()
+                w_relay(1, k).start()
+    for j in late:
+        for d in direct:
+            w_copy(d, j).start()
 
     def a_copy(d):
         return remote(att.at[d], held.at[d - 1], a_send.at[d - 1], a_recv.at[d - 1], mate(d))
 
-    with jax.named_scope("finish"):
-        for d in range(tp - 1, -1, -1):
+    def finish(mates):
+        for d in mates:
             slot = (tp - 1 - d) * rows
             outs = []
             for h in range(heads):
@@ -536,17 +568,132 @@
             if d:
                 a_copy(d).start()
 
+    def group_step(i, carry):
+        ds = jnp.where(
+            s_me == 0,
+            lax.rem(sp - i, sp),
+            jnp.where(
+                s_me == sp - 1,
+                i,
+                lax.rem(lax.rem(i, 2) * ((i + 1) // 2) + lax.rem(i + 1, 2) * (sp - i // 2), sp),
+            ),
+        )
+        source = lax.rem(s_me + sp - ds, sp)
+        with jax.named_scope("kvwait"):
+            if relay:
+                for k in range(2):
+                    kv_relay(ds, k).wait_recv()
+            else:
+                for d in direct:
+                    kv_mate(ds, d).wait_recv()
+        with jax.named_scope("kvexpand"):
+            a, b = stacked([tables(source, d, kgain, kgain_swap) for d in range(tp)])
+            tails = [kv[ds, d, pl.ds(rows, ROPE_DIM // pieces), :] for d in range(tp)]
+            ropes = [
+                jnp.concatenate([t[:, p * rows : (p + 1) * rows] for p in range(pieces)], axis=0) for t in tails
+            ]
+
+            def store(h, k, v):
+                k_buf[h] = k
+                v_buf[h] = v
+
+            expand([kv[ds, d, pl.ds(0, rows), :] for d in range(tp)], ropes, a, b, store)
+
+        @pl.when(i < sp - 1)
+        def _():
+            with jax.named_scope("attend"):
+                attend(range(0, group, q_rows), k_buf, v_buf, 0, group, False, False)
+
+        @pl.when(i == sp - 1)
+        def _():
+            with jax.named_scope("attendlast"):
+                count = q_rows // rows
+                for start in range(0, group, q_rows):
+                    attend([start], k_buf, v_buf, 0, group, False, False)
+                    top_mate = tp - 1 - start // rows
+                    finish(range(top_mate, top_mate - count, -1))
+
+        if sp > 3:
+
+            @pl.when(i < sp - 3)
+            def _():
+                with jax.named_scope("relaywait"):
+                    n = i + 3
+                    step = lax.rem(n, 2) * ((n + 1) // 2) + lax.rem(n + 1, 2) * (sp - n // 2)
+                    kv_relays(jnp.where(s_me == 0, sp - n, jnp.where(s_me == sp - 1, n, step)))
+
+        @pl.when(i == 0)
+        def _():
+            with jax.named_scope("w0"):
+                if relay and pair > 1:
+                    w_arrive(3, 0)
+                    z_copy(3).start()
+
+        if far_keys:
+
+            @pl.when(i == 1)
+            def _():
+                with jax.named_scope("ctxwait4"):
+                    for k in range(4, sp + 1):
+                        ctx_phase(k)
+                with jax.named_scope("ctxexpand"):
+                    expand_context(near, sp - near)
+                with jax.named_scope("ctxattend"):
+                    attend(range(0, group, q_rows), k_ctx, v_ctx, near_keys, far_keys, True, False)
+
+        @pl.when(i == min(1, sp - 2))
+        def _():
+            with jax.named_scope("wlate"):
+                if relay:
+                    for j in late:
+                        for k in range(2):
+                            w_copy(1 + k, j).wait_recv()
+                            w_relay(j, k).start()
+
+        @pl.when(i == sp - 2)
+        def _():
+            with jax.named_scope("w1"):
+                for d in range(1, tp):
+                    for j in range(len(mine)):
+                        if j in early or (relay and d < 3):
+                            if relay and d == 3 and (j == 1 or pair == 1):
+                                w_arrive(d, j)
+                            if not relay and not (j == 0 and pair > 1):
+                                w_arrive(d, j)
+                            for e in range(1, dp):
+                                x_copy(d, e, j).start()
+                    if pair > 1 and d < 3:
+                        z_copy(d).wait_recv()
+                        for e in range(1, dp):
+                            x_copy(d, e, len(mine)).start()
+
+        return carry
+
+    lax.fori_loop(0, sp, group_step, 0)
+
+    with jax.named_scope("wtwin"):
+        for d in range(1, tp):
+            for j in late:
+                if not relay or d == 3:
+                    w_arrive(d, j)
+                    for e in range(1, dp):
+                        x_copy(d, e, j).start()
+            if pair > 1 and d >= 3:
+                z_copy(d).wait_recv()
+                for e in range(1, dp):
+                    x_copy(d, e, len(mine)).start()
+
     with jax.named_scope("tail"):
         chunk = 512
         spans = [slice(n * chunk, (n + 1) * chunk) for n in range(width // chunk)]
         mixed = [
             jnp.dot(att[0], w_all[0, :, cols], preferred_element_type=F32).astype(BF16).astype(F32) for cols in spans
         ]
-        for d in range(1, tp):
+        for d in list(range(2, tp)) + [1]:
             with jax.named_scope("xwait"):
                 for e in range(1, dp):
-                    for k in range(pair):
-                        x_copy(d, e, k).wait_recv()
+                    for j in range(4):
+                        x_copy(d, e, j).wait_recv()
             with jax.named_scope("await"):
                 a_copy(d).wait_recv()
             for n, cols in enumerate(spans):
@@ -575,17 +722,26 @@
                 for cp in ctx_down(k):
                     cp.wait_send()
 
+        for d in direct:
+            q_copy(d).wait_send()
+            for j in range(len(mine)):
+                w_copy(d, j).wait_send()
+            for ds in range(sp):
+                kv_mate(ds, d).wait_send()
+        if relay:
+            for k in range(2):
+                q_relay(k).wait_send()
+                for j in range(len(mine)):
+                    w_relay(j, k).wait_send()
+                for ds in range(sp):
+                    kv_relay(ds, k).wait_send()
         for d in range(1, tp):
-            q_copy(d).wait_send()
             a_copy(d).wait_send()
-            w_copy(d).wait_send()
             if pair > 1:
                 z_copy(d).wait_send()
             for e in range(1, dp):
-                for k in range(pair):
-                    x_copy(d, e, k).wait_send()
-            for ds in range(sp):
-                kv_mate(ds, d).wait_send()
+                for j in range(4):
+                    x_copy(d, e, j).wait_send()
         for ds in range(1, sp):
             kv_column(ds).wait_send()
 
@@ -615,7 +771,7 @@
     return pl.pallas_call(
         functools.partial(fused_kernel, sp, tp, dp, heads),
         out_shape=pltpu.VMEM((rows, width), BF16),
-        in_specs=[VMEM_SPEC] * 6 + [pl.BlockSpec(memory_space=pltpu.SMEM)] + [VMEM_SPEC] * 5 + [HBM_SPEC] * 16,
+        in_specs=[pl.BlockSpec(memory_space=pltpu.SMEM)] + [HBM_SPEC] * 27,
         out_specs=VMEM_SPEC,
         scratch_shapes=[
             vmem((n_dev, 2 * width // tp // LANES, LANES), F32),
@@ -652,15 +808,27 @@
             vmem((q_rank, heads * LANES), BF16),
             vmem((rank, heads * LANES), BF16),
             vmem((rank, heads * LANES), BF16),
-            dma((16,)),
+            vmem(condition.shape, BF16),
+            vmem((1, width), F32),
+            vmem((1, q_rank), F32),
+            vmem((1, rank), F32),
+            vmem((1, QK_DIM), F32),
+            vmem((1, QK_DIM), F32),
+            vmem(row_a.shape, F32),
+            vmem(row_a.shape, F32),
+            vmem(col_a.shape, F32),
+            vmem(col_a.shape, F32),
+            vmem((ROPE_DIM, LANES), BF16),
+            dma((27,)),
             dma((n_dev - 1,)), dma((n_dev - 1,)),
             dma((n_dev - 1,)), dma((n_dev - 1,)),
+            dma((tp,)), dma((tp,)),
+            dma((sp, tp + 1)), dma((sp, tp + 1)),
+            dma((2, 2 * sp)), dma((2, sp)),
+            dma((tp - 1, 4)), dma((tp - 1, 4)),
+            dma((4, 2)), dma((4, 2)),
             dma((tp - 1,)), dma((tp - 1,)),
-            dma((sp, tp)), dma((sp, tp)),
-            dma((2, 2 * sp)), dma((2, sp)),
-            dma((tp - 1,)), dma((tp - 1,)),
-            dma((tp - 1,)), dma((tp - 1,)),
-            dma((2 * (tp - 1) * (dp - 1),)), dma((2 * (tp - 1) * (dp - 1),)),
+            dma(((tp - 1) * (dp - 1), 4)), dma(((tp - 1) * (dp - 1), 4)),
             dma((tp - 1,)), dma((tp - 1,)),
         ]
         + [vmem((group, LANES), F32)] * (2 * heads),
@@ -669,8 +837,8 @@
         ),
         name="fused",
     )(
-        condition, norm_gain[None], query_gain[None], kv_gain[None], query_norm_gain[None], key_norm_gain[None],
-        context_lift, jnp.asarray(row_a), jnp.asarray(row_b), jnp.asarray(col_a), jnp.asarray(col_b),
+        context_lift, condition, norm_gain[None], query_gain[None], kv_gain[None], query_norm_gain[None],
+        key_norm_gain[None], jnp.asarray(row_a), jnp.asarray(row_b), jnp.asarray(col_a), jnp.asarray(col_b),
         jnp.asarray(rope_spread(), BF16),
         shift_weight, scale_weight, gate_weight, latent_tokens, query_down, kv_down, rope_down.T,
         context_latent, context_rope.T, query_up, key_up, value_up, q_spread, k_spread, v_spread, out_weight,

time: 53.7 us -> 47.7 us (0.89)
  Pallas kernels: 52.7 us -> 46.7 us
    pallas_call x1, Pallas kernels: 52.7 us -> 46.7 us  [local(): pl.pallas_call(functools.partial(fused_kernel, sp, tp, dp, heads), out_sh...]
where the time goes in v3:
time: 47.7 us; the launch traced here: 47.5 us
  Pallas kernels  46.7 us (98%)
  local copies, waits for them, and re-layouts  0.8 us (2%)
    pallas_call x1, Pallas kernels, local(): pl.pallas_call(functools.partial(fused_kernel, sp, tp, dp, heads), out_sh...  46.7 us

profile of v3, /device:TPU:0, one launch (start us, length us, event | category | flops | bytes accessed | tf_op | source)
XLA Modules:
  0.0 47.5 jit_solution(2755286830749489740)
XLA Ops:
  0.0 46.7 %fused.1 = bf16[128,2048]{1,0:T(8,128)(2,1)S(1)} custom-call(f32[4]{0:T(128)} %lift_ref.1, bf16[512]{0:T(512)(128)(2,1)} %cond_hbm.1, f32[1,2048]{1,0:T(1,128)} %bitcast.9, f32[1,512]{1,0:T(1,128)} %bitcast.10, f32[1,256]{1,0:T(1,128)} %bitcast.11, f32[1,96]{1,0:T(1,128)} %bitcast.12, f32[1,96]{1,0:T(1,128)} %bitcast.13, ...), custom_call_target="tpu_custom_call" | custom-call | tf_op jit(solution)/shard_map/fused/pallas_call | solution.py:771
  46.7 0.8 %copy.30 = bf16[128,2048]{1,0:T(8,128)(2,1)} copy(bf16[128,2048]{1,0:T(8,128)(2,1)S(1)} %fused.1) | data formatting | bytes 1048576

commit v4 on v3

--- a/solution.py
+++ b/solution.py
@@ -115,7 +115,7 @@
     ctx_rows = cl_hbm.shape[0]
     pair = 2 - sp % 2
     share = w_hbm.shape[0] // dp
-    unit = share // 4
+    unit = share // 8
     relay = tp == 4
     direct = range(1, 3) if relay else range(1, tp)
     width = w_hbm.shape[1]
@@ -185,15 +185,14 @@
         c = cond_ref[...].reshape(1, cond_ref.shape[0]).astype(F32)
         act = (c / (1.0 + jnp.exp(-c))).astype(BF16)
         act = jnp.broadcast_to(act, (16, act.shape[1]))
-        terms = []
-        for i, w in enumerate((shift_w, scale_w, gate_w)):
+
+        def product(i, w):
             first[i].wait()
-            if i == 2:
-                w_load, small_load, token_load, up_load, down_load = later_loads()
             term = jnp.dot(act, w[...], preferred_element_type=F32)[0:1]
-            terms.append([term[:, c : c + LANES] for c in range(0, term.shape[1], LANES)])
-        mods[me] = jnp.concatenate(terms[0] + terms[1], axis=0)
-        gates[me] = jnp.concatenate(terms[2], axis=0)
+            return [term[:, c : c + LANES] for c in range(0, term.shape[1], LANES)]
+
+        mods[me] = jnp.concatenate(product(0, shift_w) + product(1, scale_w), axis=0)
+        w_load, small_load, token_load, up_load, down_load = later_loads()
         for cp in ctx_load:
             cp.wait()
 
@@ -251,10 +250,13 @@
 
     parity = lax.rem(s_me, pair)
     base = d_me * share
-    mine = [parity * 3 * unit, unit, 2 * unit] if pair > 1 else [k * unit for k in range(4)]
-
-    def w_rows(offset):
-        return pl.ds(pl.multiple_of(base + offset, unit), unit)
+    mine = [(parity * 5 * unit, 3 * unit), (3 * unit, 2 * unit)]
+    if pair == 1:
+        mine = [(0, 3 * unit), (3 * unit, 2 * unit), (5 * unit, 3 * unit)]
+
+    def w_rows(piece):
+        offset, size = piece
+        return pl.ds(pl.multiple_of(base + offset, unit), size)
 
     def w_copy(d, j):
         span = w_rows(mine[j])
@@ -273,7 +275,7 @@
         return remote(w_all.at[d, span], w_all.at[d, span], z_send.at[d - 1], z_recv.at[d - 1], device)
 
     def x_copy(d, e, j):
-        span = w_rows(mine[j] if j < len(mine) else (1 - parity) * 3 * unit)
+        span = w_rows(mine[j] if j < len(mine) else ((1 - parity) * 5 * unit, 3 * unit))
         i = (d - 1) * (dp - 1) + e - 1
         return remote(w_all.at[d, span], w_all.at[d, span], x_send.at[i, j], x_recv.at[i, j], twin(e))
 
@@ -284,13 +286,12 @@
         else:
             w_copy(d, j).wait_recv()
 
-    early = range(2)
-    late = range(2, len(mine))
     w_load.wait()
     for d in direct:
         w_copy(d, 0).start()
 
     with jax.named_scope("prep"):
+        gates[me] = jnp.concatenate(product(2, gate_w), axis=0)
         for cp in small_load:
             cp.wait()
         gains[...] = jnp.zeros(gains.shape, F32)
@@ -421,9 +422,10 @@
                 (v[:, h * LANES : (h + 1) * LANES] + ones_lane).astype(BF16),
             )
 
-    def attend(starts, k_ref, v_ref, first_key, keys, lift, fresh):
+    def attend(starts, k_ref, v_ref, first_key, keys, lift, fresh, count=None):
+        count = count or q_rows
         key_span = pl.ds(first_key, keys)
-        items = [(pl.ds(start, q_rows), h) for start in starts for h in range(heads)]
+        items = [(pl.ds(start, count), h) for start in starts for h in range(heads)]
 
         def product(span, h):
             return lax.dot_general(q_all[h, span, :], k_ref[h, key_span, :], contract, preferred_element_type=F32)
@@ -439,7 +441,7 @@
                 lift_h = lift_ref[h] * LOG2E
                 peak = peak + lift_h
             if fresh:
-                top = jnp.broadcast_to(peak, (q_rows, LANES))
+                top = jnp.broadcast_to(peak, (count, LANES))
             else:
                 old = top_refs[h][span, :]
                 top = jnp.maximum(old, peak)
@@ -490,69 +492,39 @@
     far_keys = (sp - near) * ctx_rows
     q_rows = 2 * rows if tp % 2 == 0 else rows
 
-    with jax.named_scope("ctxwait"):
-        ctx_phase(2)
-    with jax.named_scope("ctxexpand"):
-        expand_context(0, near)
-    def kv_relays(ds):
+    def kv_relays(i):
+        ds = source_step(i) if i else 0
         if relay:
-            for k in range(2):
-                kv_mate(ds, 1 + k).wait_recv()
-                kv_relay(ds, k).start()
-
-    def queries_attend(first_mate):
-        mates = list(range(first_mate + q_rows // rows - 1, first_mate - 1, -1))
-        with jax.named_scope("queries"):
-            queries(mates)
-        with jax.named_scope("ctxattend"):
-            attend([(tp - 1 - mates[0]) * rows], k_ctx, v_ctx, 0, near_keys, True, True)
-
-    with jax.named_scope("qwait"):
-        for d in direct:
-            q_copy(d).wait_recv()
-            if relay:
-                q_relay(d - 1).start()
-        if relay:
-            for k in range(2):
-                w_copy(1 + k, 0).wait_recv()
-                w_relay(0, k).start()
-    for d in direct:
-        w_copy(d, 1).start()
-    queries_attend(0)
-    with jax.named_scope("kvwait0"):
-        kv_relays(0)
-    with jax.named_scope("zwait"):
-        for i in range(1, sp):
-            ds = source_step(i)
+            with jax.named_scope(f"relay{i}"):
+                for k in range(2):
+                    kv_mate(ds, 1 + k).wait_recv()
+                    kv_relay(ds, k).start()
+
+    def kv_forward(i):
+        ds = source_step(i)
+        with jax.named_scope(f"forward{i}"):
             kv_column(ds).wait_recv()
             for d in direct:
                 kv_mate(ds, d).start()
-    for i in range(len(others)):
-        gate_copy(i).start()
-    with jax.named_scope("qwait3"):
+
+    def w_relays(j):
         if relay:
-            for k in range(2):
-                q_relay(k).wait_recv()
-    for first_mate in range(q_rows // rows, tp, q_rows // rows):
-        queries_attend(first_mate)
-    with jax.named_scope("ctxwait3"):
-        ctx_phase(3)
-    if pair > 1:
-        with jax.named_scope("pairwait"):
-            for d in direct:
-                if not relay:
-                    w_copy(d, 0).wait_recv()
+            with jax.named_scope(f"wrelay{j}"):
+                for k in range(2):
+                    if j:
+                        w_copy(1 + k, j).wait_recv()
+                    w_relay(j, k).start()
+
+    def z_start(d):
+        if pair > 1:
+            with jax.named_scope(f"zstart{d}"):
+                if d not in direct:
+                    w_arrive(d, 0)
                 z_copy(d).start()
-    with jax.named_scope("relaywait"):
-        for i in range(1, min(3, sp)):
-            kv_relays(source_step(i))
-        if relay:
-            for k in range(2):
-                w_copy(1 + k, 1).wait_recv()
-                w_relay(1, k).start()
-    for j in late:
-        for d in direct:
-            w_copy(d, j).start()
+
+    def context_attend(mates):
+        with jax.named_scope("ctxattend"):
+            attend([(tp - 1 - mates[0]) * rows], k_ctx, v_ctx, 0, near_keys, True, True, len(mates) * rows)
 
     def a_copy(d):
         return remote(att.at[d], held.at[d - 1], a_send.at[d - 1], a_recv.at[d - 1], mate(d))
@@ -568,27 +540,25 @@
             if d:
                 a_copy(d).start()
 
-    def group_step(i, carry):
-        ds = jnp.where(
-            s_me == 0,
-            lax.rem(sp - i, sp),
-            jnp.where(
-                s_me == sp - 1,
-                i,
-                lax.rem(lax.rem(i, 2) * ((i + 1) // 2) + lax.rem(i + 1, 2) * (sp - i // 2), sp),
-            ),
-        )
-        source = lax.rem(s_me + sp - ds, sp)
-        with jax.named_scope("kvwait"):
-            if relay:
-                for k in range(2):
-                    kv_relay(ds, k).wait_recv()
-            else:
-                for d in direct:
+    order = [(i, 0) for i in range(sp)]
+    if relay:
+        order += [(i, d) for i in range(sp) for d in direct] + [(i, 3) for i in range(sp)]
+    else:
+        order += [(i, d) for i in range(1, sp) for d in direct] + [(0, d) for d in direct]
+    chunks = [order[c : c + tp] for c in range(0, len(order), tp)]
+
+    def chunk_keys(c):
+        blocks = [(source_step(i) if i else 0, i, d) for i, d in chunks[c]]
+        with jax.named_scope(f"kvwait{c}"):
+            for ds, i, d in blocks:
+                if relay and d == 3:
+                    for k in range(2):
+                        kv_relay(ds, k).wait_recv()
+                elif d and not relay:
                     kv_mate(ds, d).wait_recv()
         with jax.named_scope("kvexpand"):
-            a, b = stacked([tables(source, d, kgain, kgain_swap) for d in range(tp)])
-            tails = [kv[ds, d, pl.ds(rows, ROPE_DIM // pieces), :] for d in range(tp)]
+            a, b = stacked([tables(lax.rem(s_me + sp - ds, sp), d, kgain, kgain_swap) for ds, i, d in blocks])
+            tails = [kv[ds, d, pl.ds(rows, ROPE_DIM // pieces), :] for ds, i, d in blocks]
             ropes = [
                 jnp.concatenate([t[:, p * rows : (p + 1) * rows] for p in range(pieces)], axis=0) for t in tails
             ]
@@ -597,42 +567,66 @@
                 k_buf[h] = k
                 v_buf[h] = v
 
-            expand([kv[ds, d, pl.ds(0, rows), :] for d in range(tp)], ropes, a, b, store)
-
-        @pl.when(i < sp - 1)
-        def _():
-            with jax.named_scope("attend"):
-                attend(range(0, group, q_rows), k_buf, v_buf, 0, group, False, False)
-
-        @pl.when(i == sp - 1)
-        def _():
-            with jax.named_scope("attendlast"):
-                count = q_rows // rows
-                for start in range(0, group, q_rows):
-                    attend([start], k_buf, v_buf, 0, group, False, False)
-                    top_mate = tp - 1 - start // rows
-                    finish(range(top_mate, top_mate - count, -1))
-
-        if sp > 3:
-
-            @pl.when(i < sp - 3)
-            def _():
-                with jax.named_scope("relaywait"):
-                    n = i + 3
-                    step = lax.rem(n, 2) * ((n + 1) // 2) + lax.rem(n + 1, 2) * (sp - n // 2)
-                    kv_relays(jnp.where(s_me == 0, sp - n, jnp.where(s_me == sp - 1, n, step)))
-
-        @pl.when(i == 0)
-        def _():
-            with jax.named_scope("w0"):
-                if relay and pair > 1:
-                    w_arrive(3, 0)
-                    z_copy(3).start()
-
-        if far_keys:
-
-            @pl.when(i == 1)
-            def _():
+            expand([kv[ds, d, pl.ds(0, rows), :] for ds, i, d in blocks], ropes, a, b, store)
+
+    def chunk_attend():
+        with jax.named_scope("attend"):
+            attend(range(0, group, q_rows), k_buf, v_buf, 0, group, False, False)
+
+    with jax.named_scope("queries"):
+        queries([0])
+    with jax.named_scope("ctxwait"):
+        ctx_phase(2, depart=False)
+    with jax.named_scope("ctxexpand"):
+        expand_context(0, near)
+    context_attend([0])
+    with jax.named_scope("qwait"):
+        for d in direct:
+            q_copy(d).wait_recv()
+            if relay:
+                q_relay(d - 1).start()
+    ctx_phase(2, arrive=False)
+    for d in direct:
+        w_copy(d, 0).wait_recv()
+    z_start(1)
+    with jax.named_scope("queries"):
+        queries(list(reversed(direct)))
+    kv_relays(0)
+    for i in range(1, min(2, sp)):
+        kv_forward(i)
+    context_attend(list(reversed(direct)))
+    if relay:
+        with jax.named_scope("qwait3"):
+            for k in range(2):
+                q_relay(k).wait_recv()
+        with jax.named_scope("queries"):
+            queries([3])
+        context_attend([3])
+    for i in range(2, sp):
+        kv_forward(i)
+    w_relays(0)
+    def swap_twin(d, j):
+        for e in range(1, dp):
+            x_copy(d, e, j).start()
+
+    def swap_pair(d):
+        if pair > 1:
+            z_copy(d).wait_recv()
+            swap_twin(d, len(mine))
+
+    last = len(chunks) - 1
+    relayed = [1]
+
+    def relays_to(i):
+        while relay and relayed[0] <= i:
+            kv_relays(relayed[0])
+            relayed[0] += 1
+
+    for c in range(len(chunks)):
+        if c:
+            relays_to(sp - 1 if any(d == 3 for i, d in chunks[c]) else max(i for i, d in chunks[c]))
+        if c == last:
+            if far_keys:
                 with jax.named_scope("ctxwait4"):
                     for k in range(4, sp + 1):
                         ctx_phase(k)
@@ -640,48 +634,54 @@
                     expand_context(near, sp - near)
                 with jax.named_scope("ctxattend"):
                     attend(range(0, group, q_rows), k_ctx, v_ctx, near_keys, far_keys, True, False)
-
-        @pl.when(i == min(1, sp - 2))
-        def _():
-            with jax.named_scope("wlate"):
-                if relay:
-                    for j in late:
-                        for k in range(2):
-                            w_copy(1 + k, j).wait_recv()
-                            w_relay(j, k).start()
-
-        @pl.when(i == sp - 2)
-        def _():
-            with jax.named_scope("w1"):
-                for d in range(1, tp):
-                    for j in range(len(mine)):
-                        if j in early or (relay and d < 3):
-                            if relay and d == 3 and (j == 1 or pair == 1):
-                                w_arrive(d, j)
-                            if not relay and not (j == 0 and pair > 1):
-                                w_arrive(d, j)
-                            for e in range(1, dp):
-                                x_copy(d, e, j).start()
-                    if pair > 1 and d < 3:
-                        z_copy(d).wait_recv()
-                        for e in range(1, dp):
-                            x_copy(d, e, len(mine)).start()
-
-        return carry
-
-    lax.fori_loop(0, sp, group_step, 0)
+            if relay:
+                for j in range(1, len(mine)):
+                    w_relays(j)
+                    for d in direct:
+                        swap_twin(d, j)
+            with jax.named_scope("pair1"):
+                swap_pair(1)
+        chunk_keys(c)
+        if c < last:
+            chunk_attend()
+        if c == 0:
+            with jax.named_scope("ctxwait3"):
+                ctx_phase(3)
+            for d in direct:
+                if d > 1:
+                    z_start(d)
+        if c == min(1, last):
+            relays_to(sp - 1)
+            for j in range(1, len(mine)):
+                for d in direct:
+                    w_copy(d, j).start()
+            for i in range(len(others)):
+                gate_copy(i).start()
+            for d in range(1, tp):
+                if d in direct:
+                    swap_twin(d, 0)
+        if c == max(min(1, last), last - 1):
+            for d in range(1, tp):
+                if d not in direct:
+                    z_start(d)
+
+    with jax.named_scope("attendlast"):
+        for mates in [list(range(tp - 1, 1, -1)), [1], [0]]:
+            attend([(tp - 1 - mates[0]) * rows], k_buf, v_buf, 0, group, False, False, len(mates) * rows)
+            finish(mates)
 
     with jax.named_scope("wtwin"):
         for d in range(1, tp):
-            for j in late:
-                if not relay or d == 3:
+            for j in range(len(mine)):
+                if d not in direct:
+                    if j or pair == 1:
+                        w_arrive(d, j)
+                    swap_twin(d, j)
+                elif j and not relay:
                     w_arrive(d, j)
-                    for e in range(1, dp):
-                        x_copy(d, e, j).start()
-            if pair > 1 and d >= 3:
-                z_copy(d).wait_recv()
-                for e in range(1, dp):
-                    x_copy(d, e, len(mine)).start()
+                    swap_twin(d, j)
+            if d > 1:
+                swap_pair(d)
 
     with jax.named_scope("tail"):
         chunk = 512
@@ -692,7 +692,7 @@
         for d in list(range(2, tp)) + [1]:
             with jax.named_scope("xwait"):
                 for e in range(1, dp):
-                    for j in range(4):
+                    for j in range(3):
                         x_copy(d, e, j).wait_recv()
             with jax.named_scope("await"):
                 a_copy(d).wait_recv()
@@ -740,7 +740,7 @@
             if pair > 1:
                 z_copy(d).wait_send()
             for e in range(1, dp):
-                for j in range(4):
+                for j in range(3):
                     x_copy(d, e, j).wait_send()
         for ds in range(1, sp):
             kv_column(ds).wait_send()

time: 47.7 us -> 44.6 us (0.935)
  Pallas kernels: 46.7 us -> 43.6 us
    pallas_call x1, Pallas kernels: 46.7 us -> 43.6 us  [local(): pl.pallas_call(functools.partial(fused_kernel, sp, tp, dp, heads), out_sh...]
where the time goes in v4:
time: 44.6 us; the launch traced here: 44.4 us
  Pallas kernels  43.6 us (98%)
  local copies, waits for them, and re-layouts  0.8 us (2%)
    pallas_call x1, Pallas kernels, local(): pl.pallas_call(functools.partial(fused_kernel, sp, tp, dp, heads), out_sh...  43.6 us

profile of v4, /device:TPU:0, one launch (start us, length us, event | category | flops | bytes accessed | tf_op | source)
XLA Modules:
  0.0 44.4 jit_solution(7179476101991573282)
XLA Ops:
  0.0 43.6 %fused.1 = bf16[128,2048]{1,0:T(8,128)(2,1)S(1)} custom-call(f32[4]{0:T(128)} %lift_ref.1, bf16[512]{0:T(512)(128)(2,1)} %cond_hbm.1, f32[1,2048]{1,0:T(1,128)} %bitcast.9, f32[1,512]{1,0:T(1,128)} %bitcast.10, f32[1,256]{1,0:T(1,128)} %bitcast.11, f32[1,96]{1,0:T(1,128)} %bitcast.12, f32[1,96]{1,0:T(1,128)} %bitcast.13, ...), custom_call_target="tpu_custom_call" | custom-call | tf_op jit(solution)/shard_map/fused/pallas_call | solution.py:771
  43.6 0.8 %copy.30 = bf16[128,2048]{1,0:T(8,128)(2,1)} copy(bf16[128,2048]{1,0:T(8,128)(2,1)S(1)} %fused.1) | data formatting | bytes 1048576

commit v5 on v4

--- a/solution.py
+++ b/solution.py
@@ -92,7 +92,7 @@
 
 def fused_kernel(
     sp, tp, dp, heads,
-    lift_ref, cond_hbm, gain_hbm, qg_hbm, kg_hbm, qgain_hbm, kgain_hbm, row_a_hbm, row_b_hbm, col_a_hbm, col_b_hbm,
+    lift_hbm, cond_hbm, gain_hbm, qg_hbm, kg_hbm, qgain_hbm, kgain_hbm, row_a_hbm, row_b_hbm, col_a_hbm, col_b_hbm,
     spread_hbm,
     shift_hbm, scale_hbm, gate_hbm, tokens_hbm, qd_hbm, kd_hbm, rd_hbm, cl_hbm, cr_hbm,
     qu_hbm, ku_hbm, vu_hbm, qe_hbm, ke_hbm, ve_hbm, w_hbm,
@@ -100,7 +100,7 @@
     mods, gates, q_lat, kv, ctx, ctx_rope, gate_buf, tab_a, tab_b, gains, q_all, k_buf, v_buf, k_ctx, v_ctx, att, held,
     w_all, shift_w, scale_w, gate_w, tokens_ref, qd_ref, kd_ref, rd_ref,
     qu_raw, ku_raw, vu_raw, qe_ref, ke_ref, ve_ref, qu_ref, ku_ref, vu_ref,
-    cond_ref, gain_ref, qg_ref, kg_ref, qgain_ref, kgain_ref, row_a, row_b, col_a, col_b, spread_ref,
+    lift_ref, cond_ref, gain_ref, qg_ref, kg_ref, qgain_ref, kgain_ref, row_a, row_b, col_a, col_b, spread_ref,
     load_sem, mod_send, mod_recv, g_send, g_recv, q_send, q_recv, kv_send, kv_recv, c_send, c_recv, w_send, w_recv,
     r_send, r_recv, z_send, z_recv, x_send, x_recv, a_send, a_recv, *state,
 ):
@@ -143,7 +143,7 @@
             for i, (src, dst) in enumerate((
                 (gain_hbm, gain_ref), (qg_hbm, qg_ref), (kg_hbm, kg_ref), (qgain_hbm, qgain_ref),
                 (kgain_hbm, kgain_ref), (row_a_hbm, row_a), (row_b_hbm, row_b), (col_a_hbm, col_a),
-                (col_b_hbm, col_b), (spread_hbm, spread_ref),
+                (col_b_hbm, col_b), (spread_hbm, spread_ref), (lift_hbm, lift_ref),
             ))
         ]
         token_load = load(6, tokens_hbm, tokens_ref)
@@ -297,6 +297,8 @@
         gains[...] = jnp.zeros(gains.shape, F32)
         gains[0:1, :QK_DIM] = qgain_ref[...]
         gains[1:2, :QK_DIM] = kgain_ref[...]
+        for h in range(heads):
+            gains[2 + h : 3 + h, :] = jnp.broadcast_to(lift_ref[0:1, h : h + 1] * LOG2E, (1, LANES))
         lane = lax.broadcasted_iota(jnp.int32, (1, LANES), 1)
         freq = ROPE_DIM // 4
         low = lax.rem(lane, 2 * freq) < freq
@@ -334,13 +336,17 @@
     with jax.named_scope("waitmods"):
         for cp in mod_copies:
             cp.wait_recv()
-    def q_copy(d):
-        return remote(q_lat.at[0], q_lat.at[d], q_send.at[d - 1], q_recv.at[d - 1], mate(d))
+    q_half = q_lat.shape[2] // 2
+
+    def q_copy(d, k):
+        cols = pl.ds(k * q_half, q_half)
+        i = (d - 1) * 2 + k
+        return remote(q_lat.at[0, :, cols], q_lat.at[d, :, cols], q_send.at[i], q_recv.at[i], mate(d))
 
     def q_relay(k):
-        cols = pl.ds(k * (q_lat.shape[2] // 2), q_lat.shape[2] // 2)
+        cols = pl.ds(k * q_half, q_half)
         return remote(
-            q_lat.at[1 + k, :, cols], q_lat.at[3, :, cols], q_send.at[2 + k], q_recv.at[2 + k], mate(2 - k)
+            q_lat.at[1 + k, :, cols], q_lat.at[3, :, cols], q_send.at[4 + k], q_recv.at[4 + k], mate(2 - k)
         )
 
     with jax.named_scope("stageB"):
@@ -364,8 +370,9 @@
         normed = (xn * (1.0 + scale) + shift).astype(BF16)
         q = jnp.dot(normed, qd_ref[...], preferred_element_type=F32)
         q_lat[0] = (q * norm_factor(q) * qg_ref[...]).astype(BF16)
-        for d in direct:
-            q_copy(d).start()
+        for k in range(2):
+            for d in direct:
+                q_copy(d, (d - 1 + k) % 2).start()
         lat = jnp.dot(normed, kd_ref[...], preferred_element_type=F32)
         kv[0, 0, :rows, :] = (lat * norm_factor(lat) * kg_ref[...]).astype(BF16)
         rope = lax.dot_general(
@@ -398,9 +405,6 @@
 
     for i in range(1, sp):
         kv_column(target_step(i)).start()
-    for d in direct:
-        kv_mate(0, d).start()
-
     contract = (((1,), (1,)), ((), ()))
 
     def expand(lats, ropes, a, b, store):
@@ -422,10 +426,9 @@
                 (v[:, h * LANES : (h + 1) * LANES] + ones_lane).astype(BF16),
             )
 
-    def attend(starts, k_ref, v_ref, first_key, keys, lift, fresh, count=None):
-        count = count or q_rows
+    def attend(parts_of, k_ref, v_ref, first_key, keys, lift, fresh, after=None):
         key_span = pl.ds(first_key, keys)
-        items = [(pl.ds(start, count), h) for start in starts for h in range(heads)]
+        items = [(pl.ds(*part), h) for part in parts_of for h in range(heads)]
 
         def product(span, h):
             return lax.dot_general(q_all[h, span, :], k_ref[h, key_span, :], contract, preferred_element_type=F32)
@@ -433,15 +436,16 @@
         ahead = 2
         scores = [product(*item) for item in items[:ahead]]
         for i, (span, h) in enumerate(items):
+            count = span.size
             if i + ahead < len(items):
                 scores.append(product(*items[i + ahead]))
             s = scores[i]
             peak = jnp.max(s, axis=-1, keepdims=True)
             if lift:
-                lift_h = lift_ref[h] * LOG2E
+                lift_h = gains[2 + h : 3 + h, :]
                 peak = peak + lift_h
             if fresh:
-                top = jnp.broadcast_to(peak, (count, LANES))
+                top = jnp.broadcast_to(peak, (count, LANES)) if not lift else peak
             else:
                 old = top_refs[h][span, :]
                 top = jnp.maximum(old, peak)
@@ -452,6 +456,8 @@
                 add = acc_refs[h][span, :] * jnp.exp2(old - top) + add
             top_refs[h][span, :] = top
             acc_refs[h][span, :] = add
+            if after and h == heads - 1:
+                after(i // heads)
 
     def expand_context(first, count):
         slots = []
@@ -522,9 +528,14 @@
                     w_arrive(d, 0)
                 z_copy(d).start()
 
+    def mate_rows(mates):
+        return (tp - 1 - mates[0]) * rows, len(mates) * rows
+
+    all_rows = [(start, q_rows) for start in range(0, group, q_rows)]
+
     def context_attend(mates):
         with jax.named_scope("ctxattend"):
-            attend([(tp - 1 - mates[0]) * rows], k_ctx, v_ctx, 0, near_keys, True, True, len(mates) * rows)
+            attend([mate_rows(mates)], k_ctx, v_ctx, 0, near_keys, True, True)
 
     def a_copy(d):
         return remote(att.at[d], held.at[d - 1], a_send.at[d - 1], a_recv.at[d - 1], mate(d))
@@ -571,29 +582,33 @@
 
     def chunk_attend():
         with jax.named_scope("attend"):
-            attend(range(0, group, q_rows), k_buf, v_buf, 0, group, False, False)
+            attend(all_rows, k_buf, v_buf, 0, group, False, False)
 
     with jax.named_scope("queries"):
         queries([0])
     with jax.named_scope("ctxwait"):
-        ctx_phase(2, depart=False)
+        ctx_phase(2)
     with jax.named_scope("ctxexpand"):
         expand_context(0, near)
     context_attend([0])
     with jax.named_scope("qwait"):
         for d in direct:
-            q_copy(d).wait_recv()
+            q_copy(d, (d - 1) % 2).wait_recv()
             if relay:
                 q_relay(d - 1).start()
-    ctx_phase(2, arrive=False)
+        for d in direct:
+            kv_mate(0, d).start()
+    with jax.named_scope("qwait2"):
+        for d in direct:
+            q_copy(d, d % 2).wait_recv()
     for d in direct:
         w_copy(d, 0).wait_recv()
     z_start(1)
     with jax.named_scope("queries"):
         queries(list(reversed(direct)))
-    kv_relays(0)
     for i in range(1, min(2, sp)):
         kv_forward(i)
+    w_relays(0)
     context_attend(list(reversed(direct)))
     if relay:
         with jax.named_scope("qwait3"):
@@ -604,7 +619,7 @@
         context_attend([3])
     for i in range(2, sp):
         kv_forward(i)
-    w_relays(0)
+    kv_relays(0)
     def swap_twin(d, j):
         for e in range(1, dp):
             x_copy(d, e, j).start()
@@ -632,8 +647,12 @@
                         ctx_phase(k)
                 with jax.named_scope("ctxexpand"):
                     expand_context(near, sp - near)
+            for d in range(1, tp):
+                if d not in direct:
+                    z_start(d)
+            if far_keys:
                 with jax.named_scope("ctxattend"):
-                    attend(range(0, group, q_rows), k_ctx, v_ctx, near_keys, far_keys, True, False)
+                    attend(all_rows, k_ctx, v_ctx, near_keys, far_keys, True, False)
             if relay:
                 for j in range(1, len(mine)):
                     w_relays(j)
@@ -642,16 +661,16 @@
             with jax.named_scope("pair1"):
                 swap_pair(1)
         chunk_keys(c)
-        if c < last:
-            chunk_attend()
         if c == 0:
             with jax.named_scope("ctxwait3"):
                 ctx_phase(3)
             for d in direct:
                 if d > 1:
                     z_start(d)
+        if c < last:
+            chunk_attend()
         if c == min(1, last):
-            relays_to(sp - 1)
+            relays_to(min(2, sp - 1))
             for j in range(1, len(mine)):
                 for d in direct:
                     w_copy(d, j).start()
@@ -660,15 +679,13 @@
             for d in range(1, tp):
                 if d in direct:
                     swap_twin(d, 0)
-        if c == max(min(1, last), last - 1):
-            for d in range(1, tp):
-                if d not in direct:
-                    z_start(d)
 
     with jax.named_scope("attendlast"):
-        for mates in [list(range(tp - 1, 1, -1)), [1], [0]]:
-            attend([(tp - 1 - mates[0]) * rows], k_buf, v_buf, 0, group, False, False, len(mates) * rows)
-            finish(mates)
+        turns = [list(range(tp - 1, 1, -1)), [1], [0]]
+        attend(
+            [mate_rows(mates) for mates in turns], k_buf, v_buf, 0, group, False, False,
+            lambda i: finish(turns[i]),
+        )
 
     with jax.named_scope("wtwin"):
         for d in range(1, tp):
@@ -723,7 +740,8 @@
                     cp.wait_send()
 
         for d in direct:
-            q_copy(d).wait_send()
+            for k in range(2):
+                q_copy(d, k).wait_send()
             for j in range(len(mine)):
                 w_copy(d, j).wait_send()
             for ds in range(sp):
@@ -771,7 +789,7 @@
     return pl.pallas_call(
         functools.partial(fused_kernel, sp, tp, dp, heads),
         out_shape=pltpu.VMEM((rows, width), BF16),
-        in_specs=[pl.BlockSpec(memory_space=pltpu.SMEM)] + [HBM_SPEC] * 27,
+        in_specs=[HBM_SPEC] * 28,
         out_specs=VMEM_SPEC,
         scratch_shapes=[
             vmem((n_dev, 2 * width // tp // LANES, LANES), F32),
@@ -783,7 +801,7 @@
             vmem((1, width), F32),
             vmem((tokens, LANES), F32),
             vmem((tokens, LANES), F32),
-            vmem((8, LANES), F32),
+            vmem((8 * ((heads + 9) // 8), LANES), F32),
             vmem((heads, group, LANES), BF16),
             vmem((heads, group, LANES), BF16),
             vmem((heads, group, LANES), BF16),
@@ -808,6 +826,7 @@
             vmem((q_rank, heads * LANES), BF16),
             vmem((rank, heads * LANES), BF16),
             vmem((rank, heads * LANES), BF16),
+            vmem((1, heads), F32),
             vmem(condition.shape, BF16),
             vmem((1, width), F32),
             vmem((1, q_rank), F32),
@@ -819,10 +838,10 @@
             vmem(col_a.shape, F32),
             vmem(col_a.shape, F32),
             vmem((ROPE_DIM, LANES), BF16),
-            dma((27,)),
+            dma((28,)),
             dma((n_dev - 1,)), dma((n_dev - 1,)),
             dma((n_dev - 1,)), dma((n_dev - 1,)),
-            dma((tp,)), dma((tp,)),
+            dma((2 * tp,)), dma((2 * tp,)),
             dma((sp, tp + 1)), dma((sp, tp + 1)),
             dma((2, 2 * sp)), dma((2, sp)),
             dma((tp - 1, 4)), dma((tp - 1, 4)),
@@ -837,7 +856,7 @@
         ),
         name="fused",
     )(
-        context_lift, condition, norm_gain[None], query_gain[None], kv_gain[None], query_norm_gain[None],
+        context_lift[None], condition, norm_gain[None], query_gain[None], kv_gain[None], query_norm_gain[None],
         key_norm_gain[None], jnp.asarray(row_a), jnp.asarray(row_b), jnp.asarray(col_a), jnp.asarray(col_b),
         jnp.asarray(rope_spread(), BF16),
         shift_weight, scale_weight, gate_weight, latent_tokens, query_down, kv_down, rope_down.T,

time: 44.6 us -> 43.1 us (0.966)
  Pallas kernels: 43.6 us -> 42.1 us
    pallas_call x1, Pallas kernels: 43.6 us -> 42.1 us  [local(): pl.pallas_call(functools.partial(fused_kernel, sp, tp, dp, heads), out_sh...]
where the time goes in v5:
time: 43.1 us; the launch traced here: 42.9 us
  Pallas kernels  42.1 us (98%)
  local copies, waits for them, and re-layouts  0.8 us (2%)
    pallas_call x1, Pallas kernels, local(): pl.pallas_call(functools.partial(fused_kernel, sp, tp, dp, heads), out_sh...  42.1 us

profile of v5, /device:TPU:0, one launch (start us, length us, event | category | flops | bytes accessed | tf_op | source)
XLA Modules:
  0.0 42.9 jit_solution(10401856035189080024)
XLA Ops:
  0.0 42.1 %fused.1 = bf16[128,2048]{1,0:T(8,128)(2,1)S(1)} custom-call(f32[1,4]{1,0:T(1,128)} %bitcast.13, bf16[512]{0:T(512)(128)(2,1)} %cond_hbm.1, f32[1,2048]{1,0:T(1,128)} %bitcast.10, f32[1,512]{1,0:T(1,128)} %bitcast.11, f32[1,256]{1,0:T(1,128)} %bitcast.12, f32[1,96]{1,0:T(1,128)} %bitcast.14, f32[1,96]{1,0:T(1,128)} %bitcast.15, ...), custom_call_target="tpu_custom_call" | custom-call | tf_op jit(solution)/shard_map/fused/pallas_call | solution.py:789
  42.1 0.8 %copy.30 = bf16[128,2048]{1,0:T(8,128)(2,1)} copy(bf16[128,2048]{1,0:T(8,128)(2,1)S(1)} %fused.1) | data formatting | bytes 1048576

commit v6 on v5

--- a/solution.py
+++ b/solution.py
@@ -200,11 +200,19 @@
         pl.semaphore_wait(barrier, len(others) + dp - 1)
     mod_copies = []
     for i, (ds, dt) in enumerate(others):
-        mod_copies.append(remote(mods.at[me], mods.at[me], mod_send.at[i], mod_recv.at[i], peer(ds, dt)))
+        mod_copies.append(remote(mods.at[me], mods.at[me], mod_send.at[0], mod_recv.at[0], peer(ds, dt)))
         mod_copies[-1].start()
 
     def gate_copy(i):
-        return remote(gates.at[me], gates.at[me], g_send.at[i], g_recv.at[i], peer(*others[i]))
+        return remote(gates.at[me], gates.at[me], g_send.at[0], g_recv.at[0], peer(*others[i]))
+
+    every = pl.ds(0, len(others))
+
+    def all_mods():
+        return remote(mods.at[every], mods.at[every], mod_send.at[0], mod_recv.at[0], peer(*others[0]))
+
+    def all_gates():
+        return remote(gates.at[every], gates.at[every], g_send.at[0], g_recv.at[0], peer(*others[0]))
 
     def ctx_up(k):
         device = {"sp": lax.rem(s_me + 1, sp)}
@@ -334,8 +342,7 @@
         xn = x * norm_factor(x) * gain_ref[...]
 
     with jax.named_scope("waitmods"):
-        for cp in mod_copies:
-            cp.wait_recv()
+        all_mods().wait_recv()
     q_half = q_lat.shape[2] // 2
 
     def q_copy(d, k):
@@ -433,7 +440,7 @@
         def product(span, h):
             return lax.dot_general(q_all[h, span, :], k_ref[h, key_span, :], contract, preferred_element_type=F32)
 
-        ahead = 2
+        ahead = 3
         scores = [product(*item) for item in items[:ahead]]
         for i, (span, h) in enumerate(items):
             count = span.size
@@ -608,8 +615,9 @@
         queries(list(reversed(direct)))
     for i in range(1, min(2, sp)):
         kv_forward(i)
-    w_relays(0)
     context_attend(list(reversed(direct)))
+    for i in range(2, min(3, sp)):
+        kv_forward(i)
     if relay:
         with jax.named_scope("qwait3"):
             for k in range(2):
@@ -617,9 +625,10 @@
         with jax.named_scope("queries"):
             queries([3])
         context_attend([3])
-    for i in range(2, sp):
+    for i in range(3, sp):
         kv_forward(i)
     kv_relays(0)
+    w_relays(0)
     def swap_twin(d, j):
         for e in range(1, dp):
             x_copy(d, e, j).start()
@@ -640,6 +649,10 @@
     for c in range(len(chunks)):
         if c:
             relays_to(sp - 1 if any(d == 3 for i, d in chunks[c]) else max(i for i, d in chunks[c]))
+        if c == min(1, last):
+            for j in range(1, len(mine)):
+                for d in direct:
+                    w_copy(d, j).start()
         if c == last:
             if far_keys:
                 with jax.named_scope("ctxwait4"):
@@ -650,6 +663,8 @@
             for d in range(1, tp):
                 if d not in direct:
                     z_start(d)
+                    if pair > 1:
+                        swap_twin(d, 0)
             if far_keys:
                 with jax.named_scope("ctxattend"):
                     attend(all_rows, k_ctx, v_ctx, near_keys, far_keys, True, False)
@@ -661,6 +676,11 @@
             with jax.named_scope("pair1"):
                 swap_pair(1)
         chunk_keys(c)
+        if c == last:
+            with jax.named_scope("pair2"):
+                for d in direct:
+                    if d > 1:
+                        swap_pair(d)
         if c == 0:
             with jax.named_scope("ctxwait3"):
                 ctx_phase(3)
@@ -671,9 +691,6 @@
             chunk_attend()
         if c == min(1, last):
             relays_to(min(2, sp - 1))
-            for j in range(1, len(mine)):
-                for d in direct:
-                    w_copy(d, j).start()
             for i in range(len(others)):
                 gate_copy(i).start()
             for d in range(1, tp):
@@ -693,11 +710,11 @@
                 if d not in direct:
                     if j or pair == 1:
                         w_arrive(d, j)
-                    swap_twin(d, j)
+                        swap_twin(d, j)
                 elif j and not relay:
                     w_arrive(d, j)
                     swap_twin(d, j)
-            if d > 1:
+            if d not in direct:
                 swap_pair(d)
 
     with jax.named_scope("tail"):
@@ -716,17 +733,14 @@
             for n, cols in enumerate(spans):
                 term = jnp.dot(held[d - 1], w_all[d, :, cols], preferred_element_type=F32)
                 mixed[n] = mixed[n] + term.astype(BF16).astype(F32)
-        for i in range(len(others)):
-            gate_copy(i).wait_recv()
+        all_gates().wait_recv()
         gate_buf[...] = joined(gathered(gates), 0)
         for n, cols in enumerate(spans):
             out_ref[:, cols] = (tokens_ref[:, cols].astype(F32) + gate_buf[:, cols] * mixed[n]).astype(BF16)
 
     with jax.named_scope("drain"):
-        for cp in mod_copies:
-            cp.wait_send()
-        for i in range(len(others)):
-            gate_copy(i).wait_send()
+        all_mods().wait_send()
+        all_gates().wait_send()
         for k in range(1, sp):
 
             @pl.when((s_me >= k - 1) & (s_me < sp - 1))
@@ -839,8 +853,8 @@
             vmem(col_a.shape, F32),
             vmem((ROPE_DIM, LANES), BF16),
             dma((28,)),
-            dma((n_dev - 1,)), dma((n_dev - 1,)),
-            dma((n_dev - 1,)), dma((n_dev - 1,)),
+            dma((1,)), dma((1,)),
+            dma((1,)), dma((1,)),
             dma((2 * tp,)), dma((2 * tp,)),
             dma((sp, tp + 1)), dma((sp, tp + 1)),
             dma((2, 2 * sp)), dma((2, sp)),

time: 43.1 us -> 42.5 us (0.986)
  Pallas kernels: 42.1 us -> 41.6 us
    pallas_call x1, Pallas kernels: 42.1 us -> 41.6 us  [local(): pl.pallas_call(functools.partial(fused_kernel, sp, tp, dp, heads), out_sh...]
where the time goes in v6:
time: 42.5 us; the launch traced here: 42.4 us
  Pallas kernels  41.6 us (98%)
  local copies, waits for them, and re-layouts  0.8 us (2%)
    pallas_call x1, Pallas kernels, local(): pl.pallas_call(functools.partial(fused_kernel, sp, tp, dp, heads), out_sh...  41.6 us

profile of v6, /device:TPU:0, one launch (start us, length us, event | category | flops | bytes accessed | tf_op | source)
XLA Modules:
  0.0 42.4 jit_solution(8356807681695960584)
XLA Ops:
  0.0 41.6 %fused.1 = bf16[128,2048]{1,0:T(8,128)(2,1)S(1)} custom-call(f32[1,4]{1,0:T(1,128)} %bitcast.13, bf16[512]{0:T(512)(128)(2,1)} %cond_hbm.1, f32[1,2048]{1,0:T(1,128)} %bitcast.10, f32[1,512]{1,0:T(1,128)} %bitcast.11, f32[1,256]{1,0:T(1,128)} %bitcast.12, f32[1,96]{1,0:T(1,128)} %bitcast.14, f32[1,96]{1,0:T(1,128)} %bitcast.15, ...), custom_call_target="tpu_custom_call" | custom-call | tf_op jit(solution)/shard_map/fused/pallas_call | solution.py:803
  41.6 0.8 %copy.30 = bf16[128,2048]{1,0:T(8,128)(2,1)} copy(bf16[128,2048]{1,0:T(8,128)(2,1)S(1)} %fused.1) | data formatting | bytes 1048576
